TPU v7x, 256 devices: a whole 4x4x8 slice. The times are simulated.
256 devices in a mesh: sp: 32 (over z, y), fs: 4 (over x), tp: 2 (over core).
Axes of the slice: x: 4, y: 4, z: 8, core: 2. Of those that a mesh axis runs over, the one named last changes fastest.
Arguments:
- tokens: bfloat16 [4, 24576, 2048], P('fs', 'sp', 'tp'), may hold values from -6 to 6
- in_gain: float32 [2048], replicated, may hold values from 0.1 to 1.9
- ret_query: bfloat16 [2048, 768], P(None, 'tp'), may hold values from -0.125 to 0.125
- ret_key: bfloat16 [2048, 768], P(None, 'tp'), may hold values from -0.125 to 0.125
- ret_value: bfloat16 [2048, 768], P(None, 'tp'), may hold values from -0.125 to 0.125
- att_query: bfloat16 [2048, 768], P(None, 'tp'), may hold values from -8 to 8
- att_key: bfloat16 [2048, 256], P(None, 'tp'), may hold values from -8 to 8
- att_value: bfloat16 [2048, 256], P(None, 'tp'), may hold values from -0.125 to 0.125
- log_decay: float32 [4, 12, 24576], P('fs', 'tp', 'sp'), may hold values from -1.5 to 0
- ret_gain: float32 [768], P('tp'), may hold values from 0.1 to 1.9
- sink_logit: float32 [12], P('tp'), may hold values from 1 to 5
- retentive_exit_matrix: bfloat16 [768, 2048], P('tp'), may hold values from -0.15625 to 0.15625
- out_att: bfloat16 [768, 2048], P('tp'), may hold values from -0.875 to 0.875
Outputs:
- mixed: bfloat16 [4, 24576, 2048], P('fs', ('sp', 'tp'))
All inputs are finite; a program needn't handle non-finite values.
Results may differ from a plain program's by a relative error of at most 0.0085.
Values may be sent and summed in bfloat16 or wider, within the bound.
No kernel may reach another device: no remote copies, remote signals or barrier semaphores. Data moves between devices by JAX's collectives and lax.ppermute only.
A program may use at most 128 MiB of HBM per device.

v0:
```python
import jax
import jax.numpy as jnp
from jax import lax
from jax.sharding import Mesh
from jax.sharding import PartitionSpec as P

HEAD_DIM = 64
WINDOW = 128
SP = ("sp_0", "sp_1")
SP_TP = ("sp_0", "sp_1", "tp")


EPS = 1e-06


def nothing_yet(value, identity):
    return jax.tree.map(
        lambda part, zero: jnp.zeros_like(part) + jnp.asarray(zero, part.dtype), value, identity
    )


def entering(value, axes, combine, identity):
    before = start = nothing_yet(value, identity)
    total = value
    for axis in reversed(axes):
        peers, position = (lax.axis_size(axis), lax.axis_index(axis))
        pieces = jax.tree.map(
            lambda part, kind: lax.all_gather(part.astype(kind), axis),
            total,
            (jnp.bfloat16, jnp.bfloat16),
        )
        inside, total = (start, start)
        for k in range(peers):
            passed = k < position
            total = combine(
                total, jax.tree.map(lambda part, own: part[k].astype(own.dtype), pieces, value)
            )
            inside = jax.tree.map(lambda new, old: jnp.where(passed, new, old), total, inside)
        before = combine(inside, before)
    return before


def passed_along(value, axis, by):
    peers = lax.axis_size(axis)
    pairs = [(i, i + by) for i in range(peers) if 0 <= i + by < peers]
    return lax.ppermute(value, axis, pairs)


def attend_window(query_rows, key_ext, value_ext, first_position, sinks):
    length = query_rows.shape[0]
    blocks = length // WINDOW
    heads_kv = key_ext.shape[1] // HEAD_DIM
    heads = query_rows.shape[1] // HEAD_DIM
    group = heads // heads_kv
    shaped_q = query_rows.reshape(blocks, WINDOW, heads_kv, group, HEAD_DIM)
    key_block_list = key_ext.reshape(blocks + 1, WINDOW, heads_kv, HEAD_DIM)
    value_blocks = value_ext.reshape(blocks + 1, WINDOW, heads_kv, HEAD_DIM)
    key_band = jnp.concatenate([key_block_list[:-1], key_block_list[1:]], axis=1)
    value_band = jnp.concatenate([value_blocks[:-1], value_blocks[1:]], axis=1)
    scores = jnp.einsum(
        "nqhgd,nkhd->hgnqk", shaped_q, key_band, preferred_element_type=jnp.float32
    ) * HEAD_DIM ** (-0.5)
    distance = WINDOW + jnp.arange(WINDOW)[:, None] - jnp.arange(2 * WINDOW)[None, :]
    key_position = (
        first_position
        - WINDOW
        + jnp.arange(blocks)[:, None] * WINDOW
        + jnp.arange(2 * WINDOW)[None, :]
    )
    allowed = ((distance >= 0) & (distance < WINDOW))[None] & (key_position >= 0)[:, None, :]
    scores = jnp.where(allowed, scores, -jnp.inf)
    sink_part = sinks.reshape(heads_kv, group, 1, 1, 1)
    greatest_level = jnp.maximum(jnp.max(scores, axis=-1, keepdims=True), sink_part)
    raised = jnp.exp(scores - greatest_level)
    totals = jnp.sum(raised, axis=-1, keepdims=True) + jnp.exp(sink_part - greatest_level)
    weights = (raised / totals).astype(jnp.bfloat16)
    outputs = jnp.einsum(
        "hgnqk,nkhd->nqhgd", weights, value_band, preferred_element_type=jnp.float32
    )
    return outputs.reshape(length, heads * HEAD_DIM).astype(jnp.bfloat16)


def shards(
    tokens,
    in_gain,
    ret_query,
    ret_key,
    ret_value,
    att_query,
    att_key,
    att_value,
    log_decay,
    ret_gain,
    sink_logit,
    retentive_exit_matrix,
    out_att,
):
    rows_here = tokens.shape[1]
    model_width = in_gain.shape[0]
    projections = (ret_query, ret_key, ret_value, att_query, att_key, att_value)
    wide = lax.all_gather(tokens, "tp", axis=2, tiled=True)[0].astype(jnp.float32)
    scaled = (wide * in_gain).astype(jnp.bfloat16)
    sums = tuple(
        (jnp.dot(scaled, weight, preferred_element_type=jnp.float32) for weight in projections)
    )
    sums, squares = (sums, jnp.sum(wide * wide, axis=1, keepdims=True))
    inverse = lax.rsqrt(squares / model_width + EPS)
    ret_q, ret_k, ret_v, att_q, att_k, att_v = [
        (total * inverse).astype(jnp.bfloat16) for total in sums
    ]
    rates = log_decay[0]
    heads = rates.shape[0]
    fading_multiplier = HEAD_DIM ** (-0.5)
    cumulative = jnp.cumsum(rates, axis=1)
    later = jnp.arange(rows_here)[:, None] >= jnp.arange(rows_here)[None, :]
    decay = jnp.exp(
        jnp.where(later[None], cumulative[:, :, None] - cumulative[:, None, :], -jnp.inf)
    )
    shaped_q = ret_q.reshape(rows_here, heads, HEAD_DIM)
    shaped_k = ret_k.reshape(rows_here, heads, HEAD_DIM)
    shaped_v = ret_v.reshape(rows_here, heads, HEAD_DIM)
    weights = (
        jnp.einsum("thd,shd->hts", shaped_q, shaped_k, preferred_element_type=jnp.float32)
        * fading_multiplier
        * decay
    ).astype(jnp.bfloat16)
    inner = jnp.einsum("hts,shd->thd", weights, shaped_v, preferred_element_type=jnp.float32)
    keyed = (
        shaped_k.astype(jnp.float32)
        * (jnp.exp(cumulative[:, -1:] - cumulative) * fading_multiplier).T[:, :, None]
    )
    own_state = jnp.einsum("shd,she->hde", keyed, shaped_v.astype(jnp.float32))
    total_rate = jnp.exp(cumulative[:, -1])
    tail_keys = att_k[rows_here - WINDOW :]
    trailing_values = att_v[rows_here - WINDOW :]

    def combine(earlier, later_part):
        return (
            earlier[0] * later_part[0],
            later_part[0][:, None, None] * earlier[1] + later_part[1],
        )

    identity = (jnp.ones_like(total_rate), jnp.zeros_like(own_state))
    prefix = entering((total_rate, own_state), SP, combine, identity)
    incoming = prefix[1]
    before_keys, before_values = passed_along((tail_keys, trailing_values), SP, 1)
    carried = jnp.einsum("thd,hde->the", shaped_q.astype(jnp.float32), incoming)
    retained = inner + carried * jnp.exp(cumulative).T[:, :, None]
    normed = retained * lax.rsqrt(jnp.mean(retained * retained, axis=-1, keepdims=True) + EPS)
    ret_out = (normed.reshape(rows_here, heads * HEAD_DIM) * ret_gain).astype(jnp.bfloat16)
    first_position = lax.axis_index(SP) * rows_here
    key_ext = jnp.concatenate([before_keys, att_k], axis=0)
    value_ext = jnp.concatenate([before_values, att_v], axis=0)
    att_out = attend_window(att_q, key_ext, value_ext, first_position, sink_logit)
    ret_rows, att_rows = (
        lax.all_to_all(ret_out, "tp", split_axis=0, concat_axis=1, tiled=True),
        lax.all_to_all(att_out, "tp", split_axis=0, concat_axis=1, tiled=True),
    )
    summed = jnp.dot(
        ret_rows,
        lax.all_gather(retentive_exit_matrix, "tp", axis=0, tiled=True),
        preferred_element_type=jnp.float32,
    ) + jnp.dot(
        att_rows,
        lax.all_gather(out_att, "tp", axis=0, tiled=True),
        preferred_element_type=jnp.float32,
    )
    return summed.astype(jnp.bfloat16)[None]


def solution(mesh):
    finer = Mesh(
        mesh.devices.reshape(8, 4, mesh.shape["fs"], mesh.shape["tp"]), ("sp_0", "sp_1", "fs", "tp")
    )
    placed = (
        P("fs", SP, "tp"),
        P(),
        P(None, "tp"),
        P(None, "tp"),
        P(None, "tp"),
        P(None, "tp"),
        P(None, "tp"),
        P(None, "tp"),
        P("fs", "tp", SP),
        P("tp"),
        P("tp"),
        P("tp", None),
        P("tp", None),
    )
    return jax.shard_map(
        shards, mesh=finer, in_specs=placed, out_specs=P("fs", SP_TP, None), check_vma=False
    )
```

profile of v0, /device:TPU:1, one launch (start us, length us, event | category | flops | bytes accessed | tf_op | source)
XLA Modules:
  0.0 154.9 jit_solution(6653414985704127951)
XLA Ops:
  8.9 1.7 %reduce-window.6 = f32[6,6,128]{2,1,0:T(8,128)S(1)} reduce-window(f32[6,6,128]{2,1,0:T(8,128)S(1)} %reshape.321, f32[]{:T(128)} %constant.21.clone.1), window={size=1x1x128 pad=0_0x0_0x127_0}, to_apply=%region_1.0 | reduce-window | flops 585216 | bytes 36868 | tf_op jit(solution)/shard_map/reduce-window
  13.7 9.5 %all-reduce = bf16[24]{0:T(256)(128)(2,1)S(1)} all-reduce(bf16[24]{0:T(256)(128)(2,1)S(1)} %dynamic-update-slice), channel_id=2, replica_groups=mesh['sp_0'=8,'sp_1'=4,'fs'=4,'tp'=2] {'sp_1'}, use_global_device_ids=true, to_apply=%add | all-reduce | flops 24 | bytes 96
  23.3 15.4 %all-gather.2 = bf16[8,1,6]{2,1,0:T(2,128)(2,1)S(1)} all-gather(bf16[1,1,6]{2,1,0:T(2,128)(2,1)S(1)} %fusion.133), channel_id=1, replica_groups=mesh['sp_0'=8,'sp_1'=4,'fs'=4,'tp'=2] {'sp_0'}, dimensions={0}, use_global_device_ids=true | all-gather | bytes 108 | tf_op jit(solution)/shard_map/all_gather | solution.py:28
  39.4 2.7 %fusion.1 = f32[768]{0:T(1024)S(1)} fusion(bf16[1,768,2048]{2,1,0:T(8,128)(2,1)} %all-gather.7.cloned.1.call-done), kind=kLoop, calls=%fused_computation.4 | loop fusion | flops 4717824 | bytes 3148800 | tf_op jit(solution)/shard_map/reduce_sum | solution.py:106
  43.3 1.4 collective-permute-start.1
  44.7 1.4 fusion.13
  46.2 1.4 fusion.11
  47.9 9.8 %all-gather.1 = bf16[24,64,64]{2,1,0:T(8,128)(2,1)S(1)} all-gather(bf16[6,64,64]{2,1,0:T(8,128)(2,1)S(1)} %fusion.45), channel_id=3, replica_groups=mesh['sp_0'=8,'sp_1'=4,'fs'=4,'tp'=2] {'sp_1'}, dimensions={0}, use_global_device_ids=true | all-gather | bytes 245760 | tf_op jit(solution)/shard_map/all_gather | solution.py:28
  57.9 19.8 %all_gather.32 = bf16[8,6,64,64]{3,2,1,0:T(8,128)(2,1)S(1)} all-gather(bf16[1,6,64,64]{3,2,1,0:T(8,128)(2,1)S(1)} %fusion.69), channel_id=1, replica_groups=mesh['sp_0'=8,'sp_1'=4,'fs'=4,'tp'=2] {'sp_0'}, dimensions={0}, use_global_device_ids=true | all-gather | bytes 442368 | tf_op jit(solution)/shard_map/all_gather | solution.py:28
  77.6 2.3 %fusion.12 = bf16[768,384]{0,1:T(8,128)(2,1)} fusion(bf16[2048,384]{1,0:T(8,128)(2,1)S(1)} %copy-done.6, bf16[1,768,2048]{2,1,0:T(8,128)(2,1)S(1)} %copy-done.1, f32[2048]{0:T(1024)S(1)} %copy-done.10, f32[768]{0:T(1024)S(1)} %add_rsqrt_fusion.1), kind=kOutput, calls=%fused_computation.25 | convolution fusion | flops 1213267968 | bytes 5319680 | tf_op jit(solution)/shard_map/dot_general | solution.py:104
  79.9 8.6 %fusion.8 = f32[768,6,64]{0,2,1:T(8,128)} fusion(bf16[768,6,64]{0,2,1:T(8,128)(2,1)} %bitcast.252, bf16[768,6,64]{0,2,1:T(8,128)(2,1)} %bitcast.247, bf16[768,6,64]{0,2,1:T(8,128)(2,1)} %bitcast.250, f32[6,768]{1,0:T(8,128)S(1)} %bitcast.244, pred[768,768]{1,0:T(8,128)(4,1)} %iota_compare_fusion), kind=kOutput, calls=%fused_computation.20 | convolution fusion | flops 923664384 | bytes 3557376 | tf_op jit(solution)/shard_map/hts,shd->thd/dot_general | solution.py:127
  88.5 2.2 %multiply_reduce_fusion = (f32[768,6]{0,1:T(8,128)S(1)}, f32[768,6,64]{0,2,1:T(8,128)S(1)}) fusion(f32[768,6,64]{0,2,1:T(8,128)} %fusion.8, f32[768,6]{0,1:T(8,128)S(1)} %get-tuple-element.6, bf16[768,6,64]{0,2,1:T(8,128)(2,1)} %bitcast.248, bf16[8,6,64,64]{3,2,1,0:T(8,128)(2,1)S(1)} %all_gather.32, f32[6]{0:T(128)S(1)} %get-tuple-element.15, ...), kind=kOutput, calls=%fused_computation.36 | convolution fusion | flops 40103424 | bytes 3576132 | tf_op jit(solution)/shard_map/thd,hde->the/dot_general | solution.py:147
  90.8 1.6 %reshape.323 = f32[2,384,384]{1,0,2:T(2,128)} reshape(f32[768,6,64]{0,2,1:T(8,128)S(1)} %broadcast_multiply_fusion) | data formatting | bytes 2359296 | tf_op jit(solution)/shard_map/reshape | solution.py:150
  92.5 1.4 fusion.35
  93.9 20.2 %all_to_all.32 = bf16[2,384,384]{1,2,0:T(8,128)(2,1)S(1)} all-to-all(bf16[2,384,384]{1,2,0:T(8,128)(2,1)S(1)} %fusion.35), channel_id=1, replica_groups=mesh['sp_0'=8,'sp_1'=4,'fs'=4,'tp'=2] {'tp'}, dimensions={0} | all-to-all | bytes 1179648 | tf_op jit(solution)/shard_map/all_to_all | solution.py:156
  114.0 5.1 %fusion.140 = f32[384,2048]{1,0:T(8,128)} fusion(bf16[384,768]{0,1:T(8,128)(2,1)S(1)} %bitcast.241, bf16[768,2048]{1,0:T(8,128)(2,1)} %all-gather.9.cloned.1.call-done), kind=kOutput, calls=%fused_computation.194 | convolution fusion | flops 1207959552 | bytes 6881280 | tf_op jit(solution)/shard_map/dot_general | solution.py:159
  119.2 2.3 %fusion.14 = bf16[768,384]{0,1:T(8,128)(2,1)} fusion(bf16[2048,384]{1,0:T(8,128)(2,1)S(1)} %copy-done.7, bf16[1,768,2048]{2,1,0:T(8,128)(2,1)S(1)} %copy-done.2, f32[2048]{0:T(1024)S(1)} %copy-done.10, f32[768]{0:T(1024)S(1)} %add_rsqrt_fusion.1), kind=kOutput, calls=%fused_computation.27 | convolution fusion | flops 1213267968 | bytes 5319680 | tf_op jit(solution)/shard_map/dot_general | solution.py:104
  123.2 2.4 %reshape.324 = bf16[6,128,2,3,64]{1,0,4,3,2:T(8,128)(2,1)} reshape(bf16[768,384]{0,1:T(8,128)(2,1)} %fusion.14) | data formatting | bytes 1179648 | tf_op jit(solution)/shard_map/reshape | solution.py:55
  125.6 3.3 %collective-permute-start = (bf16[128,128]{1,0:T(8,128)(2,1)S(1)}, bf16[128,128]{1,0:T(8,128)(2,1)S(1)}, u32[]{:S(2)}, u32[]{:S(2)}) collective-permute-start(bf16[128,128]{1,0:T(8,128)(2,1)S(1)} %slice.185), channel_id=1, source_target_pairs={{0,8},{8,16},{16,24},{24,32},{32,40},{40,48},{48,56},{56,64},{64,7... | collective-permute-start | bytes 98312 | tf_op jit(solution)/shard_map/ppermute | solution.py:46
  130.5 2.0 %fusion.3 = (f32[2,3,6,128]{3,1,2,0:T(4,128)S(1)}, f32[2,6,256,128,3]{3,2,4,1,0:T(8,128)S(1)}) fusion(pred[6,128,256]{1,2,0:T(8,128)(4,1)S(1)} %broadcast_and_fusion, bf16[6,128,2,3,64]{1,0,4,3,2:T(8,128)(2,1)} %reshape.324, bf16[6,128,2,64]{1,3,0,2:T(8,128)(2,1)S(1)} %copy.49, bf16[6,128,2,64]{1,3,0,2:T(8,128)(2,1)S(1)} %copy.48), kind=kOutput, calls=%fused_computation.9 | convolution fusion | flops 155315712 | bytes 5916672 | tf_op jit(solution)/shard_map/nqhgd,nkhd->hgnqk/dot_general | solution.py:60
  133.8 1.4 fusion.26
  136.9 4.6 %all-to-all-start.1 = ((bf16[2,384,384]{1,2,0:T(8,128)(2,1)}), bf16[2,384,384]{1,2,0:T(8,128)(2,1)S(1)}, u32[]{:S(2)}, u32[]{:S(2)}) async-start(bf16[2,384,384]{1,2,0:T(8,128)(2,1)} %copy.54), calls=%async_computation.1 | async-start | bytes 1179648 | tf_op jit(solution)/shard_map/all_to_all | solution.py:157
  141.6 1.4 all-to-all-done.1
  143.0 5.4 %fusion.4 = bf16[1,384,2048]{2,1,0:T(8,128)(2,1)} fusion(f32[384,2048]{1,0:T(8,128)} %fusion.140, bf16[384,768]{0,1:T(8,128)(2,1)S(1)} %bitcast.242, bf16[768,2048]{1,0:T(8,128)(2,1)} %all-gather.11.cloned.1.call-done), kind=kOutput, calls=%fused_computation.11 | convolution fusion | flops 1209532416 | bytes 8454144 | tf_op jit(solution)/shard_map/dot_general | solution.py:163
  (91 shorter events, 13.4 us)
Async XLA Ops:
  6.5 38.2 %copy-start = (bf16[2048,384]{1,0:T(8,128)(2,1)S(1)}, bf16[2048,384]{1,0:T(8,128)(2,1)}, u32[]{:S(2)}) copy-start(bf16[2048,384]{1,0:T(8,128)(2,1)} %param.16) | copy-start | bytes 4718596
  6.5 4.6 %copy-start.14 = (u32[256]{0:T(256)S(1)}, u32[256]{0:T(256)}, u32[]{:S(2)}) copy-start(u32[256]{0:T(256)} %constant.64) | copy-start | bytes 3076
  6.5 2.2 %copy-start.3 = (f32[1,6,768]{2,0,1:T(1,128)S(1)}, f32[1,6,768]{2,0,1:T(1,128)}, u32[]{:S(2)}) copy-start(f32[1,6,768]{2,0,1:T(1,128)} %param.21) | copy-start | bytes 55300
  6.5 32.3 %copy-start.11 = (f32[6]{0:T(128)S(1)}, f32[6]{0:T(128)}, u32[]{:S(2)}) copy-start(f32[6]{0:T(128)} %param.23) | copy-start | bytes 76
  6.5 32.9 %all-gather.7.cloned.1.call-start = ((), (), s32[]{:S(2)}) async-start(), calls=%async_computation.2 | async-start | bytes 4718592 | tf_op jit(solution)/shard_map/all_gather | solution.py:101
  7.3 106.8 %all-gather.9.cloned.1.call-start = ((), (), s32[]{:S(2)}) async-start(), calls=%async_computation.3 | async-start | bytes 4718592 | tf_op jit(solution)/shard_map/all_gather | solution.py:161
  8.0 34.1 %copy-start.8 = (bf16[2048,128]{1,0:T(8,128)(2,1)S(1)}, bf16[2048,128]{1,0:T(8,128)(2,1)}, u32[]{:S(2)}) copy-start(bf16[2048,128]{1,0:T(8,128)(2,1)} %param.19) | copy-start | bytes 1572868
  8.0 34.1 %copy-start.10 = (f32[2048]{0:T(1024)S(1)}, f32[2048]{0:T(1024)}, u32[]{:S(2)}) copy-start(f32[2048]{0:T(1024)} %param.14) | copy-start | bytes 24580
  8.0 133.5 %all-gather.11.cloned.1.call-start = ((), (), s32[]{:S(2)}) async-start(), calls=%async_computation.4 | async-start | bytes 4718592 | tf_op jit(solution)/shard_map/all_gather | solution.py:165
  39.4 2.8 %copy-start.1 = (bf16[1,768,2048]{2,1,0:T(8,128)(2,1)S(1)}, bf16[1,768,2048]{2,1,0:T(8,128)(2,1)}, u32[]{:S(2)}) copy-start(bf16[1,768,2048]{2,1,0:T(8,128)(2,1)} %all-gather.7.cloned.1.call-done) | copy-start | bytes 9437188
  43.3 2.9 %copy-start.5 = (bf16[2048,384]{1,0:T(8,128)(2,1)S(1)}, bf16[2048,384]{1,0:T(8,128)(2,1)}, u32[]{:S(2)}) copy-start(bf16[2048,384]{1,0:T(8,128)(2,1)} %param.17) | copy-start | bytes 4718596
  43.3 86.0 %collective-permute-start.1 = (bf16[128,128]{1,0:T(8,128)(2,1)S(1)}, bf16[128,128]{1,0:T(8,128)(2,1)S(1)}, u32[]{:S(2)}, u32[]{:S(2)}) collective-permute-start(bf16[128,128]{1,0:T(8,128)(2,1)S(1)} %slice.186), channel_id=1, source_target_pairs={{0,8},{8,16},{16,24},{24,32},{32,40},{40,48},{48,56},{56,64},{64,7... | collective-permute-start | bytes 98312 | tf_op jit(solution)/shard_map/ppermute | solution.py:46
  46.2 1.5 copy-start.12
  47.6 32.3 %copy-start.13 = (bf16[768,384]{0,1:T(8,128)(2,1)}, bf16[768,384]{0,1:T(8,128)(2,1)S(1)}, u32[]{:S(2)}) copy-start(bf16[768,384]{0,1:T(8,128)(2,1)S(1)} %fusion.11) | copy-start | bytes 1769476
  47.6 30.0 %copy-start.6 = (bf16[2048,384]{1,0:T(8,128)(2,1)S(1)}, bf16[2048,384]{1,0:T(8,128)(2,1)}, u32[]{:S(2)}) copy-start(bf16[2048,384]{1,0:T(8,128)(2,1)} %param.15) | copy-start | bytes 4718596
  90.7 1.8 %copy-start.4 = (f32[384]{0:T(512)S(1)}, f32[384]{0:T(512)}, u32[]{:S(2)}) copy-start(f32[384]{0:T(512)} %param.22) | copy-start | bytes 4612
  114.0 5.1 %copy-start.2 = (bf16[1,768,2048]{2,1,0:T(8,128)(2,1)S(1)}, bf16[1,768,2048]{2,1,0:T(8,128)(2,1)}, u32[]{:S(2)}) copy-start(bf16[1,768,2048]{2,1,0:T(8,128)(2,1)} %all-gather.7.cloned.1.call-done) | copy-start | bytes 9437188
  114.0 5.1 %copy-start.7 = (bf16[2048,384]{1,0:T(8,128)(2,1)S(1)}, bf16[2048,384]{1,0:T(8,128)(2,1)}, u32[]{:S(2)}) copy-start(bf16[2048,384]{1,0:T(8,128)(2,1)} %param.18) | copy-start | bytes 4718596
  119.2 2.3 %copy-start.9 = (bf16[2048,128]{1,0:T(8,128)(2,1)S(1)}, bf16[2048,128]{1,0:T(8,128)(2,1)}, u32[]{:S(2)}) copy-start(bf16[2048,128]{1,0:T(8,128)(2,1)} %param.20) | copy-start | bytes 1572868
  125.6 4.3 %collective-permute-start = (bf16[128,128]{1,0:T(8,128)(2,1)S(1)}, bf16[128,128]{1,0:T(8,128)(2,1)S(1)}, u32[]{:S(2)}, u32[]{:S(2)}) collective-permute-start(bf16[128,128]{1,0:T(8,128)(2,1)S(1)} %slice.185), channel_id=1, source_target_pairs={{0,8},{8,16},{16,24},{24,32},{32,40},{40,48},{48,56},{56,64},{64,7... | collective-permute-start | bytes 98312 | tf_op jit(solution)/shard_map/ppermute | solution.py:46
  136.9 6.0 %all-to-all-start.1 = ((bf16[2,384,384]{1,2,0:T(8,128)(2,1)}), bf16[2,384,384]{1,2,0:T(8,128)(2,1)S(1)}, u32[]{:S(2)}, u32[]{:S(2)}) async-start(bf16[2,384,384]{1,2,0:T(8,128)(2,1)} %copy.54), calls=%async_computation.1 | async-start | bytes 1179648 | tf_op jit(solution)/shard_map/all_to_all | solution.py:157
Sparse Core Ops, SparseCore 0:
  9.1 21.9 all-gather.6
  32.9 18.7 all-gather.8
  53.5 18.7 all-gather.10
where the time goes:
time: 156 us; the launch traced here: 155 us
  blocking collectives  74.6 us (48%)
  matrix products  34.4 us (22%)
  between operations  14.2 us (9%)
  starting transfers between devices  9.45 us (6%)
  other arithmetic  9.42 us (6%)
  local copies, waits for them, and re-layouts  9.37 us (6%)
  waiting for transfers between devices  3.52 us (2%)
    all_gather x3, blocking collectives, entering(): lax.all_gather(part.astype(kind), axis)  44.9 us
    all_to_all x1, blocking collectives, shards(): lax.all_to_all(ret_out, 'tp', split_axis=0, concat_axis=1, tiled=True)  20.2 us
    unnamed x1, blocking collectives  9.52 us
    dot_general x6, matrix products, shards(): jnp.dot(scaled, weight, preferred_element_type=jnp.float32)  9.35 us
    dot_general x1, matrix products, shards(): jnp.einsum('hts,shd->thd', weights, shaped_v, preferred_element_type=jnp....  8.58 us
    dot_general x1, matrix products, shards(): jnp.dot(att_rows, lax.all_gather(out_att, 'tp', axis=0, tiled=True), pref...  5.42 us
    dot_general x1, matrix products, shards(): jnp.dot(ret_rows, lax.all_gather(retentive_exit_matrix, 'tp', axis=0, til...  5.11 us
    ppermute x2, starting transfers between devices, passed_along(): return lax.ppermute(value, axis, pairs)  4.72 us
  transfers between devices with their start and end apart: 6, of which 1 were waited for; matrix products, arithmetic and copies ran while one was open for 31% of the time, Pallas kernels for 0%

commit v1 on v0

v1 whole, which is shorter than its diff:
```python
import functools

import jax
import jax.numpy as jnp
from jax import lax
from jax.experimental import pallas as pl
from jax.experimental.pallas import tpu as pltpu
from jax.sharding import Mesh
from jax.sharding import PartitionSpec as P

HEAD_DIM = 64
WINDOW = 128
EPS = 1e-06
SP = ("sp_0", "sp_1")
SP_TP = ("sp_0", "sp_1", "tp")
F32 = jnp.float32
BF16 = jnp.bfloat16
CHUNK = 256
STATE_ROWS = 192
LOG_ROWS = 16
PAY_ROWS = STATE_ROWS + LOG_ROWS
PAIRS = 3
LANES = 128
CONTRACT_ROWS = (((0,), (0,)), ((), ()))
CONTRACT_LANES = (((1,), (1,)), ((), ()))


def dot(a, b):
    return jnp.dot(a, b, preferred_element_type=F32)


def lane_ids(shape):
    return lax.broadcasted_iota(jnp.int32, shape, len(shape) - 1)


def row_ids(shape):
    return lax.broadcasted_iota(jnp.int32, shape, 0)


def half_mask(half, dtype):
    lanes = lane_ids((1, LANES))
    inside = (lanes < HEAD_DIM) if half == 0 else (lanes >= HEAD_DIM)
    return jnp.where(inside, 1.0, 0.0).astype(dtype)


def diagonal_mask():
    return (row_ids((LANES, LANES)) < HEAD_DIM) == (lane_ids((LANES, LANES)) < HEAD_DIM)


def split3(x):
    high = x.astype(BF16).astype(F32)
    rest = x - high
    middle = rest.astype(BF16).astype(F32)
    return high, middle, rest - middle


def call(body, grid, in_specs, out_specs, out_shape, scratch, scalars, flops, name):
    return pl.pallas_call(
        body,
        out_shape=out_shape,
        grid_spec=pltpu.PrefetchScalarGridSpec(
            num_scalar_prefetch=scalars,
            grid=grid,
            in_specs=in_specs,
            out_specs=out_specs,
            scratch_shapes=scratch,
        ),
        compiler_params=pltpu.CompilerParams(
            dimension_semantics=("arbitrary",) * len(grid), vmem_limit_bytes=48 * 2**20
        ),
        cost_estimate=pl.CostEstimate(flops=flops, transcendentals=0, bytes_accessed=1 << 20),
        name=name,
    )


def whole(shape):
    return pl.BlockSpec(shape, lambda *_: (0,) * len(shape))


def decay_body(rates_ref, row_ref, col_ref):
    heads, rows = rates_ref.shape
    row_ref[...] = jnp.zeros_like(row_ref)
    row_ref[0:heads, :] = rates_ref[...]
    total = row_ref[...]
    lanes = lane_ids(total.shape)
    step = 1
    while step < rows:
        total = total + jnp.where(lanes >= step, pltpu.roll(total, step, 1), 0.0)
        step *= 2
    row_ref[...] = total
    parts = jnp.concatenate(split3(total) + (jnp.zeros_like(total),), axis=0).astype(BF16)
    shape = (32, heads * HEAD_DIM)
    picks = (row_ids(shape) % 8 == lane_ids(shape) // HEAD_DIM).astype(F32).astype(BF16)
    col_ref[...] = lax.dot_general(parts, picks, CONTRACT_ROWS, preferred_element_type=F32)


def decays(rates):
    heads, rows = rates.shape
    return call(
        decay_body,
        (1,),
        [whole(rates.shape)],
        [whole((8, rows)), whole((rows, heads * HEAD_DIM))],
        [
            jax.ShapeDtypeStruct((8, rows), F32),
            jax.ShapeDtypeStruct((rows, heads * HEAD_DIM), F32),
        ],
        [],
        0,
        2**28,
        "decays",
    )(rates)


def scaled_block(x_ref, gain_ref):
    wide = x_ref[...].astype(F32)
    return wide, (wide * gain_ref[...]).astype(BF16)


def squares_of(wide):
    squares = wide * wide
    total = squares[:, 0:LANES]
    for start in range(LANES, wide.shape[1], LANES):
        total = total + squares[:, start : start + LANES]
    return total


def key_value_body(tp, own, peer, gain, wk, wv, col, k_out, v_out, inv_out, pay_out, acc, sq):
    step = pl.program_id(0)
    width = wk.shape[1]

    def add(x_ref):
        wide, scaled = scaled_block(x_ref, gain)
        part = squares_of(wide)
        left, right = dot(scaled, wk[...]), dot(scaled, wv[...])

        @pl.when(step == 0)
        def _():
            sq[...] = part
            acc[:, 0:width] = left
            acc[:, width:] = right

        @pl.when(step > 0)
        def _():
            sq[...] += part
            acc[:, 0:width] += left
            acc[:, width:] += right

    @pl.when(step < 2)
    def _():
        add(own)

    @pl.when(step >= 2)
    def _():
        add(peer)

    @pl.when(step == 3)
    def _():
        model_width = 4 * gain.shape[1]
        mean = jnp.sum(sq[...], axis=1, keepdims=True) / model_width
        inverse = lax.rsqrt(mean + EPS)
        inv_out[...] = jnp.broadcast_to(inverse, inv_out.shape)
        keys = (acc[:, 0:width] * inverse).astype(BF16) * jnp.asarray(HEAD_DIM**-0.5, BF16)
        values = (acc[:, width:] * inverse).astype(BF16)
        k_out[...] = keys
        v_out[...] = values
        rows = keys.shape[0]
        logs = jnp.zeros((LOG_ROWS, LANES), F32)
        places = row_ids((LOG_ROWS, LANES))
        low = lane_ids((HEAD_DIM, LANES)) < HEAD_DIM
        for p in range(PAIRS):
            lanes = slice(p * LANES, (p + 1) * LANES)
            cum = col[:, lanes]
            last = col[rows - 1 : rows, lanes]
            faded = (keys[:, lanes].astype(F32) * jnp.exp(last - cum)).astype(BF16)
            state = lax.dot_general(
                faded, values[:, lanes], CONTRACT_ROWS, preferred_element_type=F32
            )
            packed = jnp.where(low, state[0:HEAD_DIM], state[HEAD_DIM:])
            pay_out[p * HEAD_DIM : (p + 1) * HEAD_DIM, :] = packed.astype(BF16)
            for i, part in enumerate(split3(last)):
                logs = logs + jnp.where(places == 3 * p + i, part, 0.0)
        pay_out[STATE_ROWS:, :] = logs.astype(BF16)


def token_specs(rows):
    block = (rows, 512)
    return [
        pl.BlockSpec(block, lambda k, tp: (0, jnp.minimum(k, 1))),
        pl.BlockSpec(block, lambda k, tp: (0, jnp.maximum(k - 2, 0))),
        pl.BlockSpec((1, 512), lambda k, tp: (0, (2 * tp[0] + k) % 4)),
    ]


def weight_spec(width):
    return pl.BlockSpec((512, width), lambda k, tp: ((2 * tp[0] + k) % 4, 0))


def key_value(tp, own, peer, gain, wk, wv, col):
    rows, width = own.shape[0], wk.shape[1]
    return call(
        key_value_body,
        (4,),
        token_specs(rows) + [weight_spec(width), weight_spec(width), whole(col.shape)],
        [
            whole((rows, width)),
            whole((rows, width)),
            whole((rows, LANES)),
            whole((PAY_ROWS, LANES)),
        ],
        [
            jax.ShapeDtypeStruct((rows, width), BF16),
            jax.ShapeDtypeStruct((rows, width), BF16),
            jax.ShapeDtypeStruct((rows, LANES), F32),
            jax.ShapeDtypeStruct((PAY_ROWS, LANES), BF16),
        ],
        [pltpu.VMEM((rows, 2 * width), F32), pltpu.VMEM((rows, LANES), F32)],
        1,
        4 * rows * 2048 * width,
        "key_value",
    )(tp, own, peer, gain, wk, wv, col)


def rest_body(tp, own, peer, gain, w0, w1, w2, w3, inv, q_out, aq_out, akv_out, acc):
    step = pl.program_id(0)
    weights = (w0, w1, w2, w3)

    def add(x_ref):
        _, scaled = scaled_block(x_ref, gain)
        start = 0
        for w in weights:
            stop = start + w.shape[1]
            part = dot(scaled, w[...])
            lanes = slice(start, stop)

            @pl.when(step == 0)
            def _():
                acc[:, lanes] = part

            @pl.when(step > 0)
            def _():
                acc[:, lanes] += part

            start = stop

    @pl.when(step < 2)
    def _():
        add(own)

    @pl.when(step >= 2)
    def _():
        add(peer)

    @pl.when(step == 3)
    def _():
        inverse = inv[:, 0:1]
        a, b = w0.shape[1], w0.shape[1] + w1.shape[1]
        q_out[...] = (acc[:, 0:a] * inverse).astype(BF16)
        aq_out[...] = (acc[:, a:b] * inverse).astype(BF16) * jnp.asarray(HEAD_DIM**-0.5, BF16)
        akv_out[...] = (acc[:, b:] * inverse).astype(BF16)


def rest(tp, own, peer, gain, weights, inv):
    rows = own.shape[0]
    widths = [w.shape[1] for w in weights]
    shapes = [(rows, widths[0]), (rows, widths[1]), (rows, widths[2] + widths[3])]
    return call(
        rest_body,
        (4,),
        token_specs(rows) + [weight_spec(w) for w in widths] + [whole(inv.shape)],
        [whole(s) for s in shapes],
        [jax.ShapeDtypeStruct(s, BF16) for s in shapes],
        [pltpu.VMEM((rows, sum(widths)), F32)],
        1,
        2 * rows * 2048 * sum(widths),
        "rest",
    )(tp, own, peer, gain, *weights, inv)


def inner_body(q_ref, k_ref, v_ref, row_ref, col_ref, out_ref):
    pair = pl.program_id(0)
    rows = q_ref.shape[0]
    later = row_ids((CHUNK, CHUNK)) >= lane_ids((CHUNK, CHUNK))
    low = lane_ids((CHUNK, LANES)) < HEAD_DIM
    diagonal = diagonal_mask()
    masks = [half_mask(0, BF16), half_mask(1, BF16)]
    state = None
    start = None
    for begin in range(0, rows, CHUNK):
        here = slice(begin, begin + CHUNK)
        q, k, v, cum = q_ref[here, :], k_ref[here, :], v_ref[here, :], col_ref[here, :]
        parts = []
        for half in range(2):
            scores = lax.dot_general(
                q * masks[half], k, CONTRACT_LANES, preferred_element_type=F32
            )
            over = cum[:, half * HEAD_DIM : half * HEAD_DIM + 1]
            keyed = row_ref[pl.ds(2 * pair + half, 1), here]
            fade = jnp.exp(jnp.where(later, over - keyed, -jnp.inf))
            parts.append(dot((scores * fade).astype(BF16), v))
        out = jnp.where(low, parts[0], parts[1])
        end = col_ref[begin + CHUNK - 1 : begin + CHUNK, :]
        if state is not None:
            faded = (q.astype(F32) * jnp.exp(cum - start)).astype(BF16)
            out = out + dot(faded, state.astype(BF16))
        out_ref[here, :] = out
        if begin + CHUNK < rows:
            keyed = (k.astype(F32) * jnp.exp(end - cum)).astype(BF16)
            added = lax.dot_general(keyed, v, CONTRACT_ROWS, preferred_element_type=F32)
            added = jnp.where(diagonal, added, 0.0)
            state = added if state is None else state * jnp.exp(end - start) + added
            start = end


def inner(q, k, v, row, col):
    rows = q.shape[0]
    spec = pl.BlockSpec((rows, LANES), lambda p: (0, p))
    return call(
        inner_body,
        (PAIRS,),
        [spec, spec, spec, whole(row.shape), spec],
        spec,
        jax.ShapeDtypeStruct(q.shape, F32),
        [],
        0,
        3 * 2**30,
        "inner",
    )(q, k, v, row, col)


def logs_of(tile, p):
    return tile[3 * p : 3 * p + 1] + tile[3 * p + 1 : 3 * p + 2] + tile[3 * p + 2 : 3 * p + 3]


def state_of(ref, p):
    return ref[p * HEAD_DIM : (p + 1) * HEAD_DIM, :].astype(F32)


def log_tile(ref):
    return ref[STATE_ROWS:, :].astype(F32)


def row_in_tile(shape, p, row):
    return jnp.where(row_ids(shape) == p, row, 0.0)


def packed_logs(rows):
    places = row_ids((LOG_ROWS, LANES))
    logs = jnp.zeros((LOG_ROWS, LANES), F32)
    for p, row in enumerate(rows):
        for i, part in enumerate(split3(row)):
            logs = logs + jnp.where(places == 3 * p + i, part, 0.0)
    return logs.astype(BF16)


def line_body(where, own, one, two, three, before_out, log_out, pay_out):
    y = where[0]
    refs = (own, one, two, three)
    tiles = [log_tile(r) for r in refs]
    place = [(y - k + 4) % 4 for k in range(4)]
    lead = jnp.zeros((8, LANES), F32)
    totals = []
    for p in range(PAIRS):
        logs = [logs_of(t, p) for t in tiles]
        states = [state_of(r, p) for r in refs]
        total = jnp.zeros((HEAD_DIM, LANES), F32)
        before = jnp.zeros((HEAD_DIM, LANES), F32)
        between = jnp.zeros((1, LANES), F32)
        for k in range(4):
            after = jnp.zeros((1, LANES), F32)
            for j in range(4):
                if j != k:
                    after = after + jnp.where(place[j] > place[k], logs[j], 0.0)
            total = total + states[k] * jnp.exp(after)
            if k > 0:
                before = before + jnp.where(k <= y, states[k] * jnp.exp(between), 0.0)
                between = between + jnp.where(k <= y, logs[k], 0.0)
        here = slice(p * HEAD_DIM, (p + 1) * HEAD_DIM)
        before_out[here, :] = before
        lead = lead + row_in_tile((8, LANES), p, between)
        pay_out[here, :] = total.astype(BF16)
        totals.append(logs[0] + logs[1] + logs[2] + logs[3])
    log_out[...] = lead
    pay_out[STATE_ROWS:, :] = packed_logs(totals)


def column_body(where, own, one, two, before_out, log_out, pay_out):
    z = where[0]
    tiles = [log_tile(r) for r in (own, one, two)]
    lead = jnp.zeros((8, LANES), F32)
    totals = []
    for p in range(PAIRS):
        log0, log1, log2 = [logs_of(t, p) for t in tiles]
        log1 = jnp.where(z >= 1, log1, 0.0)
        log2 = jnp.where(z >= 2, log2, 0.0)
        before = jnp.where(z >= 1, state_of(one, p), 0.0)
        before = before + jnp.exp(log1) * jnp.where(z >= 2, state_of(two, p), 0.0)
        here = slice(p * HEAD_DIM, (p + 1) * HEAD_DIM)
        before_out[here, :] = before
        lead = lead + row_in_tile((8, LANES), p, log1 + log2)
        pay_out[here, :] = (state_of(own, p) + jnp.exp(log0) * before).astype(BF16)
        totals.append(log0 + log1 + log2)
    log_out[...] = lead
    pay_out[STATE_ROWS:, :] = packed_logs(totals)


def combine(body, where, payloads, name):
    return call(
        body,
        (1,),
        [whole((PAY_ROWS, LANES)) for _ in payloads],
        [whole((STATE_ROWS, LANES)), whole((8, LANES)), whole((PAY_ROWS, LANES))],
        [
            jax.ShapeDtypeStruct((STATE_ROWS, LANES), F32),
            jax.ShapeDtypeStruct((8, LANES), F32),
            jax.ShapeDtypeStruct((PAY_ROWS, LANES), BF16),
        ],
        [],
        1,
        2**26,
        name,
    )(where, *payloads)


def finish_body(
    where, q_ref, in_ref, col_ref, gain, line, line_log, column, column_log, three, six, out_ref
):
    z = where[1]
    tile3, tile6 = log_tile(three), log_tile(six)
    diagonal = diagonal_mask()
    ones = jnp.where(diagonal, 1.0, 0.0).astype(BF16)
    for p in range(PAIRS):
        here = slice(p * HEAD_DIM, (p + 1) * HEAD_DIM)
        lanes = slice(p * LANES, (p + 1) * LANES)
        far = jnp.where(z >= 3, state_of(three, p), 0.0)
        log3 = jnp.where(z >= 3, logs_of(tile3, p), 0.0)
        far = far + jnp.exp(log3) * jnp.where(z >= 6, state_of(six, p), 0.0)
        before = column[here, :] + jnp.exp(column_log[p : p + 1, :]) * far
        before = line[here, :] + jnp.exp(line_log[p : p + 1, :]) * before
        state = jnp.where(diagonal, jnp.concatenate([before, before], axis=0), 0.0).astype(BF16)
        carried = dot(q_ref[:, lanes], state) * jnp.exp(col_ref[:, lanes])
        retained = in_ref[:, lanes] + carried
        squares = retained * retained
        high = squares.astype(BF16)
        low = (squares - high.astype(F32)).astype(BF16)
        mean = (dot(high, ones) + dot(low, ones)) / HEAD_DIM
        out_ref[:, lanes] = (retained * lax.rsqrt(mean + EPS) * gain[:, lanes]).astype(BF16)


def finish(where, q, inside, col, gain, line, line_log, column, column_log, three, six):
    rows, width = q.shape
    spec = pl.BlockSpec((rows // 2, width), lambda i, w: (w[0], 0))
    small = [line, line_log, column, column_log, three, six]
    return call(
        finish_body,
        (1,),
        [spec, spec, spec, whole(gain.shape)] + [whole(s.shape) for s in small],
        whole((rows // 2, width)),
        jax.ShapeDtypeStruct((rows // 2, width), BF16),
        [],
        1,
        2**29,
        "finish",
    )(where, q, inside, col, gain, *small)


def window_body(where, q_ref, kv_ref, halo_ref, sink_ref, out_ref, ext):
    half, first = where[0], where[1]
    rows = q_ref.shape[0]
    begin = pl.multiple_of(half * rows, WINDOW)

    @pl.when(half == 0)
    def _():
        ext[0:WINDOW, :] = halo_ref[...]

    @pl.when(half == 1)
    def _():
        ext[0:WINDOW, :] = kv_ref[rows - WINDOW : rows, :]

    ext[WINDOW:, :] = kv_ref[pl.ds(begin, rows), :]
    masks = [half_mask(0, BF16), half_mask(1, BF16)]
    band = (WINDOW, 2 * WINDOW)
    distance = WINDOW + row_ids(band) - lane_ids(band)
    near = (distance >= 0) & (distance < WINDOW)
    low = lane_ids((WINDOW, LANES)) < HEAD_DIM
    heads = q_ref.shape[1] // HEAD_DIM
    group = heads // 2
    for block in range(rows // WINDOW):
        span = slice(block * WINDOW, (block + 2) * WINDOW)
        keys = ext[span, 0:LANES].astype(F32)
        values = ext[span, LANES:].astype(F32)
        keys = [keys.astype(BF16), pltpu.roll(keys, HEAD_DIM, 1).astype(BF16)]
        values = [values.astype(BF16), pltpu.roll(values, HEAD_DIM, 1).astype(BF16)]
        allowed = near
        if block == 0:
            behind = jnp.where((half == 0) & (first == 0), WINDOW, 0)
            allowed = near & (lane_ids(band) >= behind)
        here = slice(block * WINDOW, (block + 1) * WINDOW)
        outs = []
        for h in range(heads):
            lanes = slice(h // 2 * LANES, (h // 2 + 1) * LANES)
            turned = (h % 2) != (h // group)
            q = q_ref[here, lanes] * masks[h % 2]
            scores = lax.dot_general(
                q, keys[turned], CONTRACT_LANES, preferred_element_type=F32
            )
            scores = jnp.where(allowed, scores, -jnp.inf)
            sink = sink_ref[h]
            highest = jnp.maximum(jnp.max(scores, axis=1, keepdims=True), sink)
            raised = jnp.exp(scores - highest)
            total = jnp.sum(raised, axis=1, keepdims=True) + jnp.exp(sink - highest)
            weights = (raised * (1.0 / total)).astype(BF16)
            outs.append(dot(weights, values[turned]))
        for p in range(heads // 2):
            lanes = slice(p * LANES, (p + 1) * LANES)
            out_ref[here, lanes] = jnp.where(low, outs[2 * p], outs[2 * p + 1]).astype(BF16)


def window(where, q, kv, halo, sinks):
    rows, width = q.shape
    return call(
        window_body,
        (1,),
        [
            pl.BlockSpec((rows // 2, width), lambda i, w: (w[0], 0)),
            whole(kv.shape),
            whole(halo.shape),
            pl.BlockSpec(memory_space=pltpu.SMEM),
        ],
        whole((rows // 2, width)),
        jax.ShapeDtypeStruct((rows // 2, width), BF16),
        [pltpu.VMEM((rows // 2 + WINDOW, kv.shape[1]), BF16)],
        1,
        2**30,
        "window",
    )(where, q, kv, halo, sinks)


def first_exit_body(a, b, wa, wb, out):
    out[...] = dot(a[...], wa[...]) + dot(b[...], wb[...])


def last_exit_body(a, b, wa, wb, more, out):
    out[...] = (more[...] + dot(a[...], wa[...]) + dot(b[...], wb[...])).astype(BF16)


def exit_product(body, a, b, wa, wb, more, dtype, name):
    rows, width = a.shape[0], wa.shape[1]
    tile = 512
    columns = lambda n: pl.BlockSpec((n, tile), lambda j: (0, j))
    args = [a, b, wa, wb] + more
    specs = [whole(a.shape), whole(b.shape), columns(wa.shape[0]), columns(wb.shape[0])]
    return call(
        body,
        (width // tile,),
        specs + [columns(rows) for _ in more],
        columns(rows),
        jax.ShapeDtypeStruct((rows, width), dtype),
        [],
        0,
        4 * rows * a.shape[1] * width,
        name,
    )(*args)


def turned(value, axis, by):
    peers = lax.axis_size(axis)
    return lax.ppermute(value, axis, [(i, (i + by) % peers) for i in range(peers)])


def shards(
    tokens,
    in_gain,
    ret_query,
    ret_key,
    ret_value,
    att_query,
    att_key,
    att_value,
    log_decay,
    ret_gain,
    sink_logit,
    retentive_exit_matrix,
    out_att,
):
    tp = lax.axis_index("tp").astype(jnp.int32)
    y = lax.axis_index("sp_1").astype(jnp.int32)
    z = lax.axis_index("sp_0").astype(jnp.int32)
    own = tokens[0]
    gain = in_gain[None]
    peer = turned(own, "tp", 1)
    row, col = decays(log_decay[0])
    side = jnp.stack([tp])
    ret_k, ret_v, inv, payload = key_value(side, own, peer, gain, ret_key, ret_value, col)
    line_in = [payload] + [turned(payload, "sp_1", k) for k in (1, 2, 3)]
    ret_q, att_q, att_kv = rest(
        side, own, peer, gain, (ret_query, att_query, att_key, att_value), inv
    )
    peers = lax.axis_size(SP)
    halo = lax.ppermute(
        att_kv[att_kv.shape[0] - WINDOW :], SP, [(i, i + 1) for i in range(peers - 1)]
    )
    line, line_log, line_pay = combine(line_body, jnp.stack([y]), line_in, "line")
    column_in = [line_pay] + [turned(line_pay, "sp_0", k) for k in (1, 2)]
    inside = inner(ret_q, ret_k, ret_v, row, col)
    column, column_log, column_pay = combine(column_body, jnp.stack([z]), column_in, "column")
    three, six = turned(column_pay, "sp_0", 3), turned(column_pay, "sp_0", 6)
    first = z * lax.axis_size("sp_1") + y
    theirs = window(jnp.stack([1 - tp, first]), att_q, att_kv, halo, sink_logit)
    att_got = turned(theirs, "tp", 1)
    att_mine = window(jnp.stack([tp, first]), att_q, att_kv, halo, sink_logit)
    out_att_peer = turned(out_att, "tp", 1)
    exit_peer = turned(retentive_exit_matrix, "tp", 1)
    partial = exit_product(
        first_exit_body, att_mine, att_got, out_att, out_att_peer, [], F32, "att_exit"
    )
    args = (ret_q, inside, col, ret_gain[None], line, line_log, column, column_log, three, six)
    ret_got = turned(finish(jnp.stack([1 - tp, z]), *args), "tp", 1)
    ret_mine = finish(jnp.stack([tp, z]), *args)
    mixed = exit_product(
        last_exit_body,
        ret_mine,
        ret_got,
        retentive_exit_matrix,
        exit_peer,
        [partial],
        BF16,
        "ret_exit",
    )
    return mixed[None]


def solution(mesh):
    finer = Mesh(
        mesh.devices.reshape(8, 4, mesh.shape["fs"], mesh.shape["tp"]), ("sp_0", "sp_1", "fs", "tp")
    )
    placed = (
        P("fs", SP, "tp"),
        P(),
        P(None, "tp"),
        P(None, "tp"),
        P(None, "tp"),
        P(None, "tp"),
        P(None, "tp"),
        P(None, "tp"),
        P("fs", "tp", SP),
        P("tp"),
        P("tp"),
        P("tp", None),
        P("tp", None),
    )
    return jax.shard_map(
        shards, mesh=finer, in_specs=placed, out_specs=P("fs", SP_TP, None), check_vma=False
    )
```

time: 156 us -> 71 us (0.46)
  blocking collectives: 74.6 us -> 0 us
  Pallas kernels: 0 us -> 42.8 us
  matrix products: 34.4 us -> 0 us
  between operations: 14.2 us -> 0.17 us
  starting transfers between devices: 9.45 us -> 21.9 us
  other arithmetic: 9.42 us -> 0.3 us
  local copies, waits for them, and re-layouts: 9.37 us -> 3.71 us
  waiting for transfers between devices: 3.52 us -> 1.72 us
    all_gather x3 -> x0, blocking collectives: 44.9 us -> none  [entering(): lax.all_gather(part.astype(kind), axis)]
    pallas_call x0 -> x12, Pallas kernels: none -> 42.8 us  [the longest x1 12.5 us: rest(): call(rest_body, (4,), token_specs(rows) + [weight_spec(w) for w in widths...]
    dot_general x13 -> x0, matrix products: 34.4 us -> none  [the longest x6 9.35 us: shards(): jnp.dot(scaled, weight, preferred_element_type=jnp.float32)]
    all_to_all x1 -> x0, blocking collectives: 20.2 us -> none  [shards(): lax.all_to_all(ret_out, 'tp', split_axis=0, concat_axis=1, tiled=True)]
    ppermute x2 -> x13, starting transfers between devices: 4.72 us -> 21.9 us  [the longest x12 19.6 us: turned(): lax.ppermute(value, axis, [(i, (i + by) % peers) for i in range(peers)])]
    unnamed x1 -> x0, blocking collectives: 9.52 us -> none
    all_to_all x1 -> x0, starting transfers between devices: 4.62 us -> none  [shards(): lax.all_to_all(att_out, 'tp', split_axis=0, concat_axis=1, tiled=True)]
    reshape x3 -> x0, local copies, waits for them, and re-layouts: 4.07 us -> none  [the longest x1 2.43 us: attend_window(): shaped_q = query_rows.reshape(blocks, WINDOW, heads_kv, group, HEAD_DIM)]
  transfers between devices with their start and end apart: 6 -> 13, of which waited for: 1 -> 2; matrix products, arithmetic and copies ran while one was open for 31% -> 2% of each run, Pallas kernels for 0% -> 53%
where the time goes in v1:
time: 71 us; the launch traced here: 70.6 us
  Pallas kernels  42.8 us (60%)
  starting transfers between devices  21.9 us (31%)
  local copies, waits for them, and re-layouts  3.71 us (5%)
  waiting for transfers between devices  1.72 us (2%)
    ppermute x12, starting transfers between devices, turned(): lax.ppermute(value, axis, [(i, (i + by) % peers) for i in range(peers)])  19.6 us
    pallas_call x1, Pallas kernels, rest(): call(rest_body, (4,), token_specs(rows) + [weight_spec(w) for w in widths...  12.5 us
    pallas_call x2, Pallas kernels, exit_product(): call(body, (width // tile,), specs + [columns(rows) for _ in more], colum...  8.83 us
    pallas_call x1, Pallas kernels, key_value(): call(key_value_body, (4,), token_specs(rows) + [weight_spec(width), weigh...  7.6 us
    pallas_call x2, Pallas kernels, window(): call(window_body, (1,), [pl.BlockSpec((rows // 2, width), lambda i, w: (w...  7 us
    pallas_call x1, Pallas kernels, inner(): call(inner_body, (PAIRS,), [spec, spec, spec, whole(row.shape), spec], sp...  3.43 us
    unnamed x17, local copies, waits for them, and re-layouts  3.02 us
    pallas_call x2, Pallas kernels, finish(): call(finish_body, (1,), [spec, spec, spec, whole(gain.shape)] + [whole(s....  2.38 us
  transfers between devices with their start and end apart: 13, of which 2 were waited for; matrix products, arithmetic and copies ran while one was open for 2% of the time, Pallas kernels for 53%

profile of v1, /device:TPU:1, one launch (start us, length us, event | category | flops | bytes accessed | tf_op | source)
XLA Modules:
  0.0 70.6 jit_solution(9219848935854819607)
XLA Ops:
  0.0 3.2 %collective-permute-start = (bf16[768,1024]{1,0:T(8,128)(2,1)}, bf16[768,1024]{1,0:T(8,128)(2,1)}, u32[]{:S(2)}, u32[]{:S(2)}) collective-permute-start(bf16[768,1024]{1,0:T(8,128)(2,1)} %bitcast.12), channel_id=1, source_target_pairs={{0,1},{1,0},{2,3},{3,2},{4,5},{5,4},{6,7},{7,6},{8,9},{9,8},{10,11... | collective-permute-start | bytes 4718600 | tf_op jit(solution)/shard_map/ppermute | solution.py:568
  3.7 0.7 %copy.16 = f32[1,6,768]{2,1,0:T(8,128)S(1)} copy(f32[1,6,768]{2,0,1:T(1,128)} %param.21) | data formatting | bytes 36864
  4.4 0.7 broadcast_in_dim.10.gain
  5.1 0.9 %decays.1 = (f32[8,768]{1,0:T(8,128)S(1)}, f32[768,384]{1,0:T(8,128)S(1)}) custom-call(f32[6,768]{1,0:T(8,128)S(1)} %bitcast.11), custom_call_target="tpu_custom_call" | custom-call | flops 268435456 | bytes 1048576 | tf_op jit(solution)/shard_map/decays/pallas_call | solution.py:99
  6.6 1.4 %copy-done.2 = bf16[1,768,1024]{2,1,0:T(8,128)(2,1)S(1)} copy-done((bf16[1,768,1024]{2,1,0:T(8,128)(2,1)S(1)}, bf16[1,768,1024]{2,1,0:T(8,128)(2,1)}, u32[]{:S(2)}) %copy-start.2) | copy-done | bytes 1572888
  8.0 0.7 copy-done.6
  8.7 7.6 %key_value.1 = (bf16[768,384]{1,0:T(8,128)(2,1)S(1)}, bf16[768,384]{1,0:T(8,128)(2,1)S(1)}, f32[768,128]{1,0:T(8,128)S(1)}, bf16[208,128]{1,0:T(8,128)(2,1)S(1)}) custom-call(s32[1]{0:T(128)} %bitcast.tp, bf16[768,1024]{1,0:T(8,128)(2,1)S(1)} %bitcast.13, bf16[768,1024]{1,0:T(8,128)(2,1)} %collective-permute-done.peer, f32[1,2048]{1,0:T(1,128)S(1)} %bitcast.15, ...), custom_call_target="tpu_custom_call" | custom-call | flops 2415919104 | bytes 1048576 | tf_op jit(solution)/shard_map/key_value/pallas_call | solution.py:201
  16.4 2.2 %collective-permute-start.2 = (bf16[208,128]{1,0:T(8,128)(2,1)S(1)}, bf16[208,128]{1,0:T(8,128)(2,1)S(1)}, u32[]{:S(2)}, u32[]{:S(2)}) collective-permute-start(bf16[208,128]{1,0:T(8,128)(2,1)S(1)} %get-tuple-element.26.own), channel_id=1, source_target_pairs={{0,16},{8,24},{16,0},{24,8},{1,17},{9,25},{17,1},{25,9},{2,18},{10... | collective-permute-start | bytes 159752 | tf_op jit(solution)/shard_map/ppermute | solution.py:568
  18.6 1.1 %collective-permute-start.3 = (bf16[208,128]{1,0:T(8,128)(2,1)S(1)}, bf16[208,128]{1,0:T(8,128)(2,1)S(1)}, u32[]{:S(2)}, u32[]{:S(2)}) collective-permute-start(bf16[208,128]{1,0:T(8,128)(2,1)S(1)} %get-tuple-element.26.own), channel_id=1, source_target_pairs={{0,24},{8,0},{16,8},{24,16},{1,25},{9,1},{17,9},{25,17},{2,26},{10... | collective-permute-start | bytes 159752 | tf_op jit(solution)/shard_map/ppermute | solution.py:568
  19.7 12.5 %rest.1 = (bf16[768,384]{1,0:T(8,128)(2,1)S(1)}, bf16[768,384]{1,0:T(8,128)(2,1)S(1)}, bf16[768,256]{1,0:T(8,128)(2,1)S(1)}) custom-call(s32[1]{0:T(128)} %bitcast.tp, bf16[768,1024]{1,0:T(8,128)(2,1)S(1)} %bitcast.14, bf16[768,1024]{1,0:T(8,128)(2,1)} %collective-permute-done.peer, f32[1,2048]{1,0:T(1,128)S(1)} %bitcast.16, bf16[2048,384]{1,0:T(8,128)(2,1)} %w0.1, ...), custom_call_target="tpu_custom_call" | custom-call | flops 3221225472 | bytes 1048576 | tf_op jit(solution)/shard_map/rest/pallas_call | solution.py:267
  32.2 2.3 %collective-permute-start.10 = (bf16[128,256]{1,0:T(8,128)(2,1)S(1)}, bf16[128,256]{1,0:T(8,128)(2,1)S(1)}, u32[]{:S(2)}, u32[]{:S(2)}) collective-permute-start(bf16[128,256]{1,0:T(8,128)(2,1)S(1)} %slice.3), channel_id=1, source_target_pairs={{0,8},{8,16},{16,24},{24,32},{32,40},{40,48},{48,56},{56,64},{64,7... | collective-permute-start | bytes 196616 | tf_op jit(solution)/shard_map/ppermute | solution.py:600
  34.7 1.9 %collective-permute-start.4 = (bf16[208,128]{1,0:T(8,128)(2,1)S(1)}, bf16[208,128]{1,0:T(8,128)(2,1)S(1)}, u32[]{:S(2)}, u32[]{:S(2)}) collective-permute-start(bf16[208,128]{1,0:T(8,128)(2,1)S(1)} %get-tuple-element.29.own), channel_id=1, source_target_pairs={{0,32},{32,64},{64,96},{96,128},{128,160},{160,192},{192,224},{224... | collective-permute-start | bytes 159752 | tf_op jit(solution)/shard_map/ppermute | solution.py:568
  36.6 3.0 %collective-permute-start.5 = (bf16[208,128]{1,0:T(8,128)(2,1)S(1)}, bf16[208,128]{1,0:T(8,128)(2,1)S(1)}, u32[]{:S(2)}, u32[]{:S(2)}) collective-permute-start(bf16[208,128]{1,0:T(8,128)(2,1)S(1)} %get-tuple-element.29.own), channel_id=1, source_target_pairs={{0,64},{32,96},{64,128},{96,160},{128,192},{160,224},{192,0},{224,... | collective-permute-start | bytes 159752 | tf_op jit(solution)/shard_map/ppermute | solution.py:568
  39.6 3.4 %inner.1.in_ref = f32[768,384]{1,0:T(8,128)S(1)} custom-call(bf16[768,384]{1,0:T(8,128)(2,1)S(1)} %get-tuple-element.22.q_ref, bf16[768,384]{1,0:T(8,128)(2,1)S(1)} %get-tuple-element.23.k_ref, bf16[768,384]{1,0:T(8,128)(2,1)S(1)} %get-tuple-element.24.v_ref, f32[8,768]{1,0:T(8,128)S(1)} %get-tuple-element.25.row_ref, ...), custom_call_target="tpu_custom_call" | custom-call | flops 3221225472 | bytes 1048576 | tf_op jit(solution)/shard_map/inner/pallas_call | solution.py:318
  43.0 1.3 %collective-permute-done.5.two = bf16[208,128]{1,0:T(8,128)(2,1)S(1)} collective-permute-done((bf16[208,128]{1,0:T(8,128)(2,1)S(1)}, bf16[208,128]{1,0:T(8,128)(2,1)S(1)}, u32[]{:S(2)}, u32[]{:S(2)}) %collective-permute-start.5) | collective-permute-done | bytes 53280 | tf_op jit(solution)/shard_map/ppermute | solution.py:568
  44.4 2.5 %collective-permute-start.6 = (bf16[208,128]{1,0:T(8,128)(2,1)S(1)}, bf16[208,128]{1,0:T(8,128)(2,1)S(1)}, u32[]{:S(2)}, u32[]{:S(2)}) collective-permute-start(bf16[208,128]{1,0:T(8,128)(2,1)S(1)} %get-tuple-element.32), channel_id=1, source_target_pairs={{0,96},{32,128},{64,160},{96,192},{128,224},{160,0},{192,32},{224,... | collective-permute-start | bytes 159752 | tf_op jit(solution)/shard_map/ppermute | solution.py:568
  46.9 2.4 %collective-permute-start.7 = (bf16[208,128]{1,0:T(8,128)(2,1)S(1)}, bf16[208,128]{1,0:T(8,128)(2,1)S(1)}, u32[]{:S(2)}, u32[]{:S(2)}) collective-permute-start(bf16[208,128]{1,0:T(8,128)(2,1)S(1)} %get-tuple-element.32), channel_id=1, source_target_pairs={{0,192},{32,224},{64,0},{96,32},{128,64},{160,96},{192,128},{224,1... | collective-permute-start | bytes 159752 | tf_op jit(solution)/shard_map/ppermute | solution.py:568
  49.3 3.5 %window.3 = bf16[384,384]{1,0:T(8,128)(2,1)S(1)} custom-call(s32[2]{0:T(128)S(1)} %pad_add_fusion.3.where, bf16[768,384]{1,0:T(8,128)(2,1)S(1)} %get-tuple-element.33.q_ref, bf16[768,256]{1,0:T(8,128)(2,1)S(1)} %get-tuple-element.34.kv_ref, bf16[128,256]{1,0:T(8,128)(2,1)S(1)} %collective-permute-done.10.halo_ref, f32[6]{0:T(128)S(1)} %copy-done.7), custom_call_target="tpu_custom_call" | custom-call | flops 1073741824 | bytes 1048576 | tf_op jit(solution)/shard_map/window/pallas_call | solution.py:521
  52.8 2.7 %collective-permute-start.11 = (bf16[384,384]{1,0:T(8,128)(2,1)S(1)}, bf16[384,384]{1,0:T(8,128)(2,1)S(1)}, u32[]{:S(2)}, u32[]{:S(2)}) collective-permute-start(bf16[384,384]{1,0:T(8,128)(2,1)S(1)} %window.3), channel_id=1, source_target_pairs={{0,1},{1,0},{2,3},{3,2},{4,5},{5,4},{6,7},{7,6},{8,9},{9,8},{10,11... | collective-permute-start | bytes 884744 | tf_op jit(solution)/shard_map/ppermute | solution.py:568
  55.5 1.2 %finish.3 = bf16[384,384]{1,0:T(8,128)(2,1)S(1)} custom-call(s32[2]{0:T(128)S(1)} %pad_add_fusion.where, bf16[768,384]{1,0:T(8,128)(2,1)S(1)} %get-tuple-element.22.q_ref, f32[768,384]{1,0:T(8,128)S(1)} %inner.1.in_ref, f32[768,384]{1,0:T(8,128)S(1)} %get-tuple-element.20.col.col_ref, f32[1,384]{1,0:T(1,128)S(1)} %broadcast_in_dim.10.gain, ...), custom_call_target="tpu_custom_call" | custom-call | flops 536870912 | bytes 1048576 | tf_op jit(solution)/shard_map/finish/pallas_call | solution.py:454
  56.9 3.5 %window.2.a = bf16[384,384]{1,0:T(8,128)(2,1)S(1)} custom-call(s32[2]{0:T(128)S(1)} %pad_add_fusion.2.where, bf16[768,384]{1,0:T(8,128)(2,1)S(1)} %get-tuple-element.33.q_ref, bf16[768,256]{1,0:T(8,128)(2,1)S(1)} %get-tuple-element.34.kv_ref, bf16[128,256]{1,0:T(8,128)(2,1)S(1)} %collective-permute-done.10.halo_ref, f32[6]{0:T(128)S(1)} %copy-done.7), custom_call_target="tpu_custom_call" | custom-call | flops 1073741824 | bytes 1048576 | tf_op jit(solution)/shard_map/window/pallas_call | solution.py:521
  60.4 1.2 %finish.2.a = bf16[384,384]{1,0:T(8,128)(2,1)S(1)} custom-call(s32[2]{0:T(128)S(1)} %pad_add_fusion.1.where, bf16[768,384]{1,0:T(8,128)(2,1)S(1)} %get-tuple-element.22.q_ref, f32[768,384]{1,0:T(8,128)S(1)} %inner.1.in_ref, f32[768,384]{1,0:T(8,128)S(1)} %get-tuple-element.20.col.col_ref, f32[1,384]{1,0:T(1,128)S(1)} %broadcast_in_dim.10.gain, ...), custom_call_target="tpu_custom_call" | custom-call | flops 536870912 | bytes 1048576 | tf_op jit(solution)/shard_map/finish/pallas_call | solution.py:454
  61.8 3.8 %att_exit.1.more = f32[384,2048]{1,0:T(8,128)} custom-call(bf16[384,384]{1,0:T(8,128)(2,1)S(1)} %window.2.a, bf16[384,384]{1,0:T(8,128)(2,1)S(1)} %collective-permute-done.11.b, bf16[384,2048]{1,0:T(8,128)(2,1)S(1)} %copy-done.1, bf16[384,2048]{1,0:T(8,128)(2,1)S(1)} %collective-permute-done.12.wb), custom_call_target="tpu_custom_call" | custom-call | flops 1207959552 | bytes 1048576 | tf_op jit(solution)/shard_map/att_exit/pallas_call | solution.py:553
  65.6 5.1 %ret_exit.1 = bf16[384,2048]{1,0:T(8,128)(2,1)} custom-call(bf16[384,384]{1,0:T(8,128)(2,1)S(1)} %finish.2.a, bf16[384,384]{1,0:T(8,128)(2,1)S(1)} %collective-permute-done.8.b, bf16[384,2048]{1,0:T(8,128)(2,1)S(1)} %copy-done, bf16[384,2048]{1,0:T(8,128)(2,1)S(1)} %collective-permute-done.9.wb, f32[384,2048]{1,0:T(8,128)} %att_exit.1.more), custom_call_target="tpu_custom_call" | custom-call | flops 1207959552 | bytes 1048576 | tf_op jit(solution)/shard_map/ret_exit/pallas_call | solution.py:553
  (37 shorter events, 1.8 us)
Async XLA Ops:
  0.0 6.6 %collective-permute-start = (bf16[768,1024]{1,0:T(8,128)(2,1)}, bf16[768,1024]{1,0:T(8,128)(2,1)}, u32[]{:S(2)}, u32[]{:S(2)}) collective-permute-start(bf16[768,1024]{1,0:T(8,128)(2,1)} %bitcast.12), channel_id=1, source_target_pairs={{0,1},{1,0},{2,3},{3,2},{4,5},{5,4},{6,7},{7,6},{8,9},{9,8},{10,11... | collective-permute-start | bytes 4718600 | tf_op jit(solution)/shard_map/ppermute | solution.py:568
  3.2 62.4 %collective-permute-start.9 = (bf16[384,2048]{1,0:T(8,128)(2,1)}, bf16[384,2048]{1,0:T(8,128)(2,1)S(1)}, u32[]{:S(2)}, u32[]{:S(2)}) collective-permute-start(bf16[384,2048]{1,0:T(8,128)(2,1)} %wa.3), channel_id=1, source_target_pairs={{0,1},{1,0},{2,3},{3,2},{4,5},{5,4},{6,7},{7,6},{8,9},{9,8},{10,11... | collective-permute-start | bytes 4718600 | tf_op jit(solution)/shard_map/ppermute | solution.py:568
  3.2 58.4 %collective-permute-start.12 = (bf16[384,2048]{1,0:T(8,128)(2,1)}, bf16[384,2048]{1,0:T(8,128)(2,1)S(1)}, u32[]{:S(2)}, u32[]{:S(2)}) collective-permute-start(bf16[384,2048]{1,0:T(8,128)(2,1)} %wa.2), channel_id=1, source_target_pairs={{0,1},{1,0},{2,3},{3,2},{4,5},{5,4},{6,7},{7,6},{8,9},{9,8},{10,11... | collective-permute-start | bytes 4718600 | tf_op jit(solution)/shard_map/ppermute | solution.py:568
  6.6 1.4 %copy-start.2 = (bf16[1,768,1024]{2,1,0:T(8,128)(2,1)S(1)}, bf16[1,768,1024]{2,1,0:T(8,128)(2,1)}, u32[]{:S(2)}) copy-start(bf16[1,768,1024]{2,1,0:T(8,128)(2,1)} %param.13) | copy-start | bytes 4718596
  8.0 0.7 copy-start.6
  8.7 11.0 %copy-start.3 = (bf16[1,768,1024]{2,1,0:T(8,128)(2,1)S(1)}, bf16[1,768,1024]{2,1,0:T(8,128)(2,1)}, u32[]{:S(2)}) copy-start(bf16[1,768,1024]{2,1,0:T(8,128)(2,1)} %param.13) | copy-start | bytes 4718596
  8.7 11.0 %copy-start.4 = (bf16[2048,128]{1,0:T(8,128)(2,1)S(1)}, bf16[2048,128]{1,0:T(8,128)(2,1)}, u32[]{:S(2)}) copy-start(bf16[2048,128]{1,0:T(8,128)(2,1)} %w2.1) | copy-start | bytes 1572868
  8.7 11.0 %copy-start.5 = (bf16[2048,128]{1,0:T(8,128)(2,1)S(1)}, bf16[2048,128]{1,0:T(8,128)(2,1)}, u32[]{:S(2)}) copy-start(bf16[2048,128]{1,0:T(8,128)(2,1)} %w3.1) | copy-start | bytes 1572868
  16.3 15.9 %collective-permute-start.1 = (bf16[208,128]{1,0:T(8,128)(2,1)S(1)}, bf16[208,128]{1,0:T(8,128)(2,1)S(1)}, u32[]{:S(2)}, u32[]{:S(2)}) collective-permute-start(bf16[208,128]{1,0:T(8,128)(2,1)S(1)} %get-tuple-element.26.own), channel_id=1, source_target_pairs={{0,8},{8,16},{16,24},{24,0},{1,9},{9,17},{17,25},{25,1},{2,10},{10... | collective-permute-start | bytes 159752 | tf_op jit(solution)/shard_map/ppermute | solution.py:568
  16.4 18.1 %collective-permute-start.2 = (bf16[208,128]{1,0:T(8,128)(2,1)S(1)}, bf16[208,128]{1,0:T(8,128)(2,1)S(1)}, u32[]{:S(2)}, u32[]{:S(2)}) collective-permute-start(bf16[208,128]{1,0:T(8,128)(2,1)S(1)} %get-tuple-element.26.own), channel_id=1, source_target_pairs={{0,16},{8,24},{16,0},{24,8},{1,17},{9,25},{17,1},{25,9},{2,18},{10... | collective-permute-start | bytes 159752 | tf_op jit(solution)/shard_map/ppermute | solution.py:568
  18.6 15.9 %collective-permute-start.3 = (bf16[208,128]{1,0:T(8,128)(2,1)S(1)}, bf16[208,128]{1,0:T(8,128)(2,1)S(1)}, u32[]{:S(2)}, u32[]{:S(2)}) collective-permute-start(bf16[208,128]{1,0:T(8,128)(2,1)S(1)} %get-tuple-element.26.own), channel_id=1, source_target_pairs={{0,24},{8,0},{16,8},{24,16},{1,25},{9,1},{17,9},{25,17},{2,26},{10... | collective-permute-start | bytes 159752 | tf_op jit(solution)/shard_map/ppermute | solution.py:568
  32.2 17.1 %collective-permute-start.10 = (bf16[128,256]{1,0:T(8,128)(2,1)S(1)}, bf16[128,256]{1,0:T(8,128)(2,1)S(1)}, u32[]{:S(2)}, u32[]{:S(2)}) collective-permute-start(bf16[128,256]{1,0:T(8,128)(2,1)S(1)} %slice.3), channel_id=1, source_target_pairs={{0,8},{8,16},{16,24},{24,32},{32,40},{40,48},{48,56},{56,64},{64,7... | collective-permute-start | bytes 196616 | tf_op jit(solution)/shard_map/ppermute | solution.py:600
  34.7 8.3 %collective-permute-start.4 = (bf16[208,128]{1,0:T(8,128)(2,1)S(1)}, bf16[208,128]{1,0:T(8,128)(2,1)S(1)}, u32[]{:S(2)}, u32[]{:S(2)}) collective-permute-start(bf16[208,128]{1,0:T(8,128)(2,1)S(1)} %get-tuple-element.29.own), channel_id=1, source_target_pairs={{0,32},{32,64},{64,96},{96,128},{128,160},{160,192},{192,224},{224... | collective-permute-start | bytes 159752 | tf_op jit(solution)/shard_map/ppermute | solution.py:568
  36.6 7.8 %collective-permute-start.5 = (bf16[208,128]{1,0:T(8,128)(2,1)S(1)}, bf16[208,128]{1,0:T(8,128)(2,1)S(1)}, u32[]{:S(2)}, u32[]{:S(2)}) collective-permute-start(bf16[208,128]{1,0:T(8,128)(2,1)S(1)} %get-tuple-element.29.own), channel_id=1, source_target_pairs={{0,64},{32,96},{64,128},{96,160},{128,192},{160,224},{192,0},{224,... | collective-permute-start | bytes 159752 | tf_op jit(solution)/shard_map/ppermute | solution.py:568
  39.6 9.8 %copy-start.7 = (f32[6]{0:T(128)S(1)}, f32[6]{0:T(128)}, u32[]{:S(2)}) copy-start(f32[6]{0:T(128)} %sink_ref.3) | copy-start | bytes 76
  44.4 11.1 %collective-permute-start.6 = (bf16[208,128]{1,0:T(8,128)(2,1)S(1)}, bf16[208,128]{1,0:T(8,128)(2,1)S(1)}, u32[]{:S(2)}, u32[]{:S(2)}) collective-permute-start(bf16[208,128]{1,0:T(8,128)(2,1)S(1)} %get-tuple-element.32), channel_id=1, source_target_pairs={{0,96},{32,128},{64,160},{96,192},{128,224},{160,0},{192,32},{224,... | collective-permute-start | bytes 159752 | tf_op jit(solution)/shard_map/ppermute | solution.py:568
  46.9 8.6 %collective-permute-start.7 = (bf16[208,128]{1,0:T(8,128)(2,1)S(1)}, bf16[208,128]{1,0:T(8,128)(2,1)S(1)}, u32[]{:S(2)}, u32[]{:S(2)}) collective-permute-start(bf16[208,128]{1,0:T(8,128)(2,1)S(1)} %get-tuple-element.32), channel_id=1, source_target_pairs={{0,192},{32,224},{64,0},{96,32},{128,64},{160,96},{192,128},{224,1... | collective-permute-start | bytes 159752 | tf_op jit(solution)/shard_map/ppermute | solution.py:568
  52.8 8.8 %collective-permute-start.11 = (bf16[384,384]{1,0:T(8,128)(2,1)S(1)}, bf16[384,384]{1,0:T(8,128)(2,1)S(1)}, u32[]{:S(2)}, u32[]{:S(2)}) collective-permute-start(bf16[384,384]{1,0:T(8,128)(2,1)S(1)} %window.3), channel_id=1, source_target_pairs={{0,1},{1,0},{2,3},{3,2},{4,5},{5,4},{6,7},{7,6},{8,9},{9,8},{10,11... | collective-permute-start | bytes 884744 | tf_op jit(solution)/shard_map/ppermute | solution.py:568
  56.7 8.9 %collective-permute-start.8 = (bf16[384,384]{1,0:T(8,128)(2,1)S(1)}, bf16[384,384]{1,0:T(8,128)(2,1)S(1)}, u32[]{:S(2)}, u32[]{:S(2)}) collective-permute-start(bf16[384,384]{1,0:T(8,128)(2,1)S(1)} %finish.3), channel_id=1, source_target_pairs={{0,1},{1,0},{2,3},{3,2},{4,5},{5,4},{6,7},{7,6},{8,9},{9,8},{10,11... | collective-permute-start | bytes 884744 | tf_op jit(solution)/shard_map/ppermute | solution.py:568
  60.4 1.4 %copy-start.1 = (bf16[384,2048]{1,0:T(8,128)(2,1)S(1)}, bf16[384,2048]{1,0:T(8,128)(2,1)}, u32[]{:S(2)}) copy-start(bf16[384,2048]{1,0:T(8,128)(2,1)} %wa.2) | copy-start | bytes 4718596
  61.6 4.0 %copy-start = (bf16[384,2048]{1,0:T(8,128)(2,1)S(1)}, bf16[384,2048]{1,0:T(8,128)(2,1)}, u32[]{:S(2)}) copy-start(bf16[384,2048]{1,0:T(8,128)(2,1)} %wa.3) | copy-start | bytes 4718596

commit v2 on v0

v2 whole, which is shorter than its diff:
```python
import functools

import jax
import jax.numpy as jnp
from jax import lax
from jax.experimental import pallas as pl
from jax.experimental.pallas import tpu as pltpu
from jax.sharding import Mesh
from jax.sharding import PartitionSpec as P

HEAD_DIM = 64
WINDOW = 128
EPS = 1e-06
SP = ("sp_0", "sp_1")
SP_TP = ("sp_0", "sp_1", "tp")
F32 = jnp.float32
BF16 = jnp.bfloat16
CHUNK = 256
STATE_ROWS = 192
LOG_ROWS = 16
PAY_ROWS = STATE_ROWS + LOG_ROWS
PAIRS = 3
LANES = 128
CONTRACT_ROWS = (((0,), (0,)), ((), ()))
CONTRACT_LANES = (((1,), (1,)), ((), ()))


def dot(a, b):
    return jnp.dot(a, b, preferred_element_type=F32)


def lane_ids(shape):
    return lax.broadcasted_iota(jnp.int32, shape, len(shape) - 1)


def row_ids(shape):
    return lax.broadcasted_iota(jnp.int32, shape, 0)


def half_mask(half, dtype):
    lanes = lane_ids((1, LANES))
    inside = (lanes < HEAD_DIM) if half == 0 else (lanes >= HEAD_DIM)
    return jnp.where(inside, 1.0, 0.0).astype(dtype)


def diagonal_mask():
    return (row_ids((LANES, LANES)) < HEAD_DIM) == (lane_ids((LANES, LANES)) < HEAD_DIM)


def split3(x):
    high = x.astype(BF16).astype(F32)
    rest = x - high
    middle = rest.astype(BF16).astype(F32)
    return high, middle, rest - middle


def call(body, in_specs, out_specs, out_shape, scratch, scalars, flops, mib, name, grid=(1,)):
    return pl.pallas_call(
        body,
        out_shape=out_shape,
        grid_spec=pltpu.PrefetchScalarGridSpec(
            num_scalar_prefetch=scalars,
            grid=grid,
            in_specs=in_specs,
            out_specs=out_specs,
            scratch_shapes=scratch,
        ),
        compiler_params=pltpu.CompilerParams(
            dimension_semantics=("arbitrary",) * len(grid), vmem_limit_bytes=mib * 2**20
        ),
        cost_estimate=pl.CostEstimate(flops=flops, transcendentals=0, bytes_accessed=1 << 20),
        name=name,
    )


def whole(shape):
    return pl.BlockSpec(shape, lambda *_: (0,) * len(shape))


IN_HBM = pl.BlockSpec(memory_space=pltpu.HBM)
SCALE = HEAD_DIM**-0.5


def in_hbm(x):
    return pltpu.with_memory_space_constraint(x, pltpu.HBM)


def fetch_weights(weights, buffer, sems, begin):
    copies, start = [], 0
    depth = buffer.shape[0]
    for i, w in enumerate(weights):
        stop = start + w.shape[1]
        copy = pltpu.make_async_copy(
            w.at[pl.ds(begin, depth), :], buffer.at[:, start:stop], sems.at[i]
        )
        copy.start()
        copies.append(copy)
        start = stop
    return copies


def weight_columns(weights, begin, depth, start):
    pieces, left = [], 0
    for w in weights:
        for n in range(0, w.shape[1], LANES):
            if start <= left + n < start + CHUNK:
                pieces.append(w[pl.ds(begin, depth), n : n + LANES])
        left += w.shape[1]
    return jnp.concatenate(pieces, axis=1)


def squares_of(wide):
    squares = wide * wide
    total = squares[:, 0:LANES]
    for start in range(LANES, wide.shape[1], LANES):
        total = total + squares[:, start : start + LANES]
    return total


def decays(rates_ref, row_ref, col_ref):
    heads, _, rows = rates_ref.shape
    row_ref[...] = jnp.zeros_like(row_ref)
    for h in range(heads):
        row_ref[h : h + 1, :] = rates_ref[h]
    total = row_ref[...]
    lanes = lane_ids(total.shape)
    step = 1
    while step < rows:
        total = total + jnp.where(lanes >= step, pltpu.roll(total, step, 1), 0.0)
        step *= 2
    row_ref[...] = total
    parts = jnp.concatenate(split3(total) + (jnp.zeros_like(total),), axis=0).astype(BF16)
    shape = (32, heads * HEAD_DIM)
    picks = (row_ids(shape) % 8 == lane_ids(shape) // HEAD_DIM).astype(F32).astype(BF16)
    col_ref[...] = lax.dot_general(parts, picks, CONTRACT_ROWS, preferred_element_type=F32)


def own_body(tp, x_hbm, gain_hbm, rates_hbm, *refs):
    weights = refs[:6]
    first, second, sq, row, col, xbuf, gain, rates, wbuf, sbuf, sems = refs[6:]
    rows, depth = xbuf.shape
    small = pltpu.make_async_copy(rates_hbm, rates, sems.at[8])
    small.start()
    load = pltpu.make_async_copy(x_hbm, xbuf, sems.at[6])
    load.start()
    gains = pltpu.make_async_copy(gain_hbm, gain, sems.at[7])
    gains.start()
    begin = pl.multiple_of(tp[0] * depth, depth)
    copies = fetch_weights(weights, wbuf, sems, begin)
    small.wait()
    decays(rates, row, col)
    gains.wait()
    load.wait()
    scale = gain[:, pl.ds(begin, depth)]
    for m in range(0, rows, CHUNK):
        wide = xbuf[m : m + CHUNK, :].astype(F32)
        sbuf[m : m + CHUNK, :] = (wide * scale).astype(BF16)
        sq[m : m + CHUNK, :] = squares_of(wide)
    split = first.shape[1]
    groups = ((first, 0, split, copies[:4]), (second, split, wbuf.shape[1], copies[4:]))
    for out, start, stop, waits in groups:
        for copy in waits:
            copy.wait()
        for n in range(start, stop, CHUNK):
            for m in range(0, rows, CHUNK):
                out[m : m + CHUNK, n - start : n - start + CHUNK] = dot(
                    sbuf[m : m + CHUNK, :], wbuf[:, n : n + CHUNK]
                )


def own_half(tp, own, gain, rates, weights):
    rows, depth = own.shape
    widths = [w.shape[1] for w in weights]
    shapes = [
        ((rows, sum(widths[:4])), F32),
        ((rows, sum(widths[4:])), F32),
        ((rows, LANES), F32),
        ((8, rows), F32),
        ((rows, widths[0]), F32),
    ]
    return call(
        own_body,
        [IN_HBM] * 9,
        [whole(s) for s, _ in shapes],
        [jax.ShapeDtypeStruct(s, t) for s, t in shapes],
        [
            pltpu.VMEM((rows, depth), BF16),
            pltpu.VMEM(gain.shape, F32),
            pltpu.VMEM(rates.shape, F32),
            pltpu.VMEM((depth, sum(widths)), BF16),
            pltpu.VMEM((rows, depth), BF16),
            pltpu.SemaphoreType.DMA((9,)),
        ],
        1,
        2 * rows * depth * sum(widths),
        24,
        "own_half",
    )(tp, *[in_hbm(a) for a in (own, gain, rates) + weights])


def keys_body(tp, x, gain, part, sq, col, *refs):
    weights = refs[:4]
    k_out, v_out, akv_out, inv_out, scaled_out, pay_out, more_out = refs[4:]
    rows, depth = x.shape
    width = k_out.shape[1]
    begin = pl.multiple_of((1 - tp[0]) * depth, depth)
    scale = gain[:, pl.ds(begin, depth)]
    low = lane_ids((HEAD_DIM, LANES)) < HEAD_DIM
    for m in range(0, rows, CHUNK):
        here = slice(m, m + CHUNK)
        wide = x[here, :].astype(F32)
        scaled_out[here, :] = (wide * scale).astype(BF16)
        mean = jnp.sum(sq[here, :] + squares_of(wide), axis=1, keepdims=True) / (2 * depth)
        inv_out[here, :] = jnp.broadcast_to(lax.rsqrt(mean + EPS), (CHUNK, LANES))
    for m in range(0, rows, CHUNK):
        here = slice(m, m + CHUNK)
        inverse = inv_out[here, 0:1]
        scaled = scaled_out[here, :]
        for n in range(0, part.shape[1], CHUNK):
            columns = weight_columns(weights, begin, depth, n)
            total = part[here, n : n + CHUNK] + dot(scaled, columns)
            value = (total * inverse).astype(BF16)
            for j in range(n, n + CHUNK, LANES):
                piece = value[:, j - n : j - n + LANES]
                if j < width:
                    k_out[here, j : j + LANES] = piece * jnp.asarray(SCALE, BF16)
                elif j < 2 * width:
                    v_out[here, j - width : j - width + LANES] = piece
                else:
                    akv_out[here, j - 2 * width : j - 2 * width + LANES] = piece
    logs = jnp.zeros((LOG_ROWS, LANES), F32)
    places = row_ids((LOG_ROWS, LANES))
    for p in range(PAIRS):
        lanes = slice(p * LANES, (p + 1) * LANES)
        last = col[rows - 1 : rows, lanes]
        faded = (k_out[:, lanes].astype(F32) * jnp.exp(last - col[:, lanes])).astype(BF16)
        state = lax.dot_general(faded, v_out[:, lanes], CONTRACT_ROWS, preferred_element_type=F32)
        packed = jnp.where(low, state[0:HEAD_DIM], state[HEAD_DIM:]).astype(BF16)
        pay_out[p * HEAD_DIM : (p + 1) * HEAD_DIM, :] = packed
        more_out[p * HEAD_DIM : (p + 1) * HEAD_DIM, :] = packed
        for i, part3 in enumerate(split3(last)):
            logs = logs + jnp.where(places == 3 * p + i, part3, 0.0)
    pay_out[STATE_ROWS:, :] = logs.astype(BF16)
    more_out[STATE_ROWS:PAY_ROWS, :] = logs.astype(BF16)
    tail = slice(rows - WINDOW, rows)
    more_out[PAY_ROWS : PAY_ROWS + WINDOW, :] = akv_out[tail, 0:LANES]
    more_out[PAY_ROWS + WINDOW :, :] = akv_out[tail, LANES:]


def keys_half(tp, peer, gain, part, sq, col, weights):
    rows, depth = peer.shape
    widths = [w.shape[1] for w in weights]
    shapes = [
        ((rows, widths[0]), BF16),
        ((rows, widths[1]), BF16),
        ((rows, widths[2] + widths[3]), BF16),
        ((rows, LANES), F32),
        ((rows, depth), BF16),
        ((PAY_ROWS, LANES), BF16),
        ((PAY_ROWS + 2 * WINDOW, LANES), BF16),
    ]
    return call(
        keys_body,
        [whole(a.shape) for a in (peer, gain, part, sq, col) + weights],
        [whole(s) for s, _ in shapes],
        [jax.ShapeDtypeStruct(s, t) for s, t in shapes],
        [],
        1,
        2 * rows * depth * sum(widths),
        20,
        "keys_half",
    )(tp, peer, gain, part, sq, col, *weights)


def queries_body(tp, scaled, part, inv, w0, w1, q_out, aq_out):
    rows, depth = scaled.shape
    width = q_out.shape[1]
    begin = pl.multiple_of((1 - tp[0]) * depth, depth)
    for m in range(0, rows, CHUNK):
        here = slice(m, m + CHUNK)
        inverse = inv[here, 0:1]
        for n in range(0, part.shape[1], CHUNK):
            columns = weight_columns((w0, w1), begin, depth, n)
            total = part[here, n : n + CHUNK] + dot(scaled[here, :], columns)
            value = (total * inverse).astype(BF16)
            for j in range(n, n + CHUNK, LANES):
                piece = value[:, j - n : j - n + LANES]
                if j < width:
                    q_out[here, j : j + LANES] = piece
                else:
                    aq_out[here, j - width : j - width + LANES] = piece * jnp.asarray(SCALE, BF16)


def queries_half(tp, scaled, part, inv, w0, w1):
    rows, depth = scaled.shape
    shapes = [(rows, w0.shape[1]), (rows, w1.shape[1])]
    return call(
        queries_body,
        [whole(a.shape) for a in (scaled, part, inv, w0, w1)],
        [whole(s) for s in shapes],
        [jax.ShapeDtypeStruct(s, BF16) for s in shapes],
        [],
        1,
        2 * rows * depth * part.shape[1],
        16,
        "queries_half",
    )(tp, scaled, part, inv, w0, w1)


def inner_body(q_ref, k_ref, v_ref, row_ref, col_ref, out_ref):
    rows = q_ref.shape[0]
    later = row_ids((CHUNK, CHUNK)) >= lane_ids((CHUNK, CHUNK))
    low = lane_ids((CHUNK, LANES)) < HEAD_DIM
    diagonal = diagonal_mask()
    masks = [half_mask(0, BF16), half_mask(1, BF16)]
    for pair in range(PAIRS):
        lanes = slice(pair * LANES, (pair + 1) * LANES)
        state = start = None
        for begin in range(0, rows, CHUNK):
            here = slice(begin, begin + CHUNK)
            q, k, v = q_ref[here, lanes], k_ref[here, lanes], v_ref[here, lanes]
            cum = col_ref[here, lanes]
            parts = []
            for half in range(2):
                scores = lax.dot_general(
                    q * masks[half], k, CONTRACT_LANES, preferred_element_type=F32
                )
                over = cum[:, half * HEAD_DIM : half * HEAD_DIM + 1]
                keyed = row_ref[2 * pair + half : 2 * pair + half + 1, here]
                fade = jnp.exp(jnp.where(later, over - keyed, -jnp.inf))
                parts.append(dot((scores * fade).astype(BF16), v))
            out = jnp.where(low, parts[0], parts[1])
            end = col_ref[begin + CHUNK - 1 : begin + CHUNK, lanes]
            if state is not None:
                faded = (q.astype(F32) * jnp.exp(cum - start)).astype(BF16)
                out = out + dot(faded, state.astype(BF16))
            out_ref[here, lanes] = out
            if begin + CHUNK < rows:
                keyed = (k.astype(F32) * jnp.exp(end - cum)).astype(BF16)
                added = lax.dot_general(keyed, v, CONTRACT_ROWS, preferred_element_type=F32)
                added = jnp.where(diagonal, added, 0.0)
                state = added if state is None else state * jnp.exp(end - start) + added
                start = end


def inner(q, k, v, row, col):
    args = (q, k, v, row, col)
    return call(
        inner_body,
        [whole(a.shape) for a in args],
        whole(q.shape),
        jax.ShapeDtypeStruct(q.shape, F32),
        [],
        0,
        3 * 2**30,
        12,
        "inner",
    )(*args)


def logs_of(tile, p):
    return tile[3 * p : 3 * p + 1] + tile[3 * p + 1 : 3 * p + 2] + tile[3 * p + 2 : 3 * p + 3]


def state_of(ref, p):
    return ref[p * HEAD_DIM : (p + 1) * HEAD_DIM, :].astype(F32)


def log_tile(ref):
    return ref[STATE_ROWS:PAY_ROWS, :].astype(F32)


def behind(index, shifts, refs, tiles, p):
    state, log = None, None
    for shift, ref, tile in reversed(list(zip(shifts, refs, tiles))):
        here = jnp.where(index >= shift, state_of(ref, p), 0.0)
        rate = jnp.where(index >= shift, logs_of(tile, p), 0.0)
        state = here if state is None else here + jnp.exp(rate) * state
        log = rate if log is None else rate + log
    return state, log


def scan_body(shifts, where, own, *refs):
    known = len(shifts) == 2
    if known:
        near, near_log = refs[:2]
        refs = refs[2:]
    sources, (near_out, log_out, pay_out) = refs[: len(shifts)], refs[len(shifts) :]
    tiles = [log_tile(r) for r in sources]
    own_tile = log_tile(own)
    lead = jnp.zeros((8, LANES), F32)
    logs = jnp.zeros((LOG_ROWS, LANES), F32)
    places = row_ids((LOG_ROWS, LANES))
    for p in range(PAIRS):
        here = slice(p * HEAD_DIM, (p + 1) * HEAD_DIM)
        before, log = behind(where[0], shifts, sources, tiles, p)
        if known:
            before = near[here, :] + jnp.exp(near_log[p : p + 1, :]) * before
            log = near_log[p : p + 1, :] + log
        own_log = logs_of(own_tile, p)
        near_out[here, :] = before
        lead = lead + jnp.where(row_ids((8, LANES)) == p, log, 0.0)
        pay_out[here, :] = (state_of(own, p) + jnp.exp(own_log) * before).astype(BF16)
        for i, part in enumerate(split3(own_log + log)):
            logs = logs + jnp.where(places == 3 * p + i, part, 0.0)
    log_out[...] = lead
    pay_out[STATE_ROWS:, :] = logs.astype(BF16)


def scan_step(shifts, where, own, near, sources, name):
    args = [own] + near + sources
    return call(
        functools.partial(scan_body, shifts),
        [whole(a.shape) for a in args],
        [whole((STATE_ROWS, LANES)), whole((8, LANES)), whole((PAY_ROWS, LANES))],
        [
            jax.ShapeDtypeStruct((STATE_ROWS, LANES), F32),
            jax.ShapeDtypeStruct((8, LANES), F32),
            jax.ShapeDtypeStruct((PAY_ROWS, LANES), BF16),
        ],
        [],
        1,
        2**26,
        4,
        name,
    )(where, *args)


def finish_body(shifts, side, spot, q_ref, in_ref, col_ref, gain, near, near_log, *refs):
    sources, out_ref = refs[:-1], refs[-1]
    tiles = [log_tile(r) for r in sources]
    diagonal = diagonal_mask()
    ones = jnp.where(diagonal, 1.0, 0.0).astype(BF16)
    for p in range(PAIRS):
        here = slice(p * HEAD_DIM, (p + 1) * HEAD_DIM)
        lanes = slice(p * LANES, (p + 1) * LANES)
        far, _ = behind(spot[0], shifts, sources, tiles, p)
        before = near[here, :] + jnp.exp(near_log[p : p + 1, :]) * far
        state = jnp.where(diagonal, jnp.concatenate([before, before], axis=0), 0.0).astype(BF16)
        carried = dot(q_ref[:, lanes], state) * jnp.exp(col_ref[:, lanes])
        retained = in_ref[:, lanes] + carried
        squares = retained * retained
        high = squares.astype(BF16)
        rest = (squares - high.astype(F32)).astype(BF16)
        mean = (dot(high, ones) + dot(rest, ones)) / HEAD_DIM
        out_ref[:, lanes] = (retained * lax.rsqrt(mean + EPS) * gain[:, lanes]).astype(BF16)


def finish(shifts, mine, side, spot, q, inside, col, gain, near, near_log, sources):
    rows, width = q.shape
    spec = pl.BlockSpec((rows // 2, width), lambda i, t, f: (half_of(t, mine), 0))
    small = [near, near_log] + sources
    return call(
        functools.partial(finish_body, shifts),
        [spec, spec, spec, whole(gain.shape)] + [whole(s.shape) for s in small],
        whole((rows // 2, width)),
        jax.ShapeDtypeStruct((rows // 2, width), BF16),
        [],
        2,
        2**29,
        8,
        "finish",
    )(side, spot, q, inside, col, gain, *small)


def half_of(side, mine):
    return side[0] if mine else 1 - side[0]


def window_body(mine, side, spot, q_ref, kv_ref, halo_ref, sink_ref, out_ref, ext):
    half, first = half_of(side, mine), spot[0]
    rows = q_ref.shape[0]
    begin = pl.multiple_of(half * rows, WINDOW)

    @pl.when(half == 0)
    def _():
        ext[0:WINDOW, 0:LANES] = halo_ref[PAY_ROWS : PAY_ROWS + WINDOW, :]
        ext[0:WINDOW, LANES:] = halo_ref[PAY_ROWS + WINDOW :, :]

    @pl.when(half == 1)
    def _():
        ext[0:WINDOW, :] = kv_ref[rows - WINDOW : rows, :]

    ext[WINDOW:, :] = kv_ref[pl.ds(begin, rows), :]
    masks = [half_mask(0, BF16), half_mask(1, BF16)]
    heads = q_ref.shape[1] // HEAD_DIM
    group = heads // 2
    band = (2 * WINDOW, group * WINDOW)
    place = lane_ids(band) % WINDOW
    distance = WINDOW + place - row_ids(band)
    near = (distance >= 0) & (distance < WINDOW)
    spot = lane_ids((1, group * WINDOW)) // WINDOW
    for block in range(rows // WINDOW):
        span = slice(block * WINDOW, (block + 2) * WINDOW)
        keys, values = ext[span, 0:LANES], ext[span, LANES:]
        allowed = near
        if block == 0:
            behind_rows = jnp.where((half == 0) & (first == 0), WINDOW, 0)
            allowed = near & (row_ids(band) >= behind_rows)
        here = slice(block * WINDOW, (block + 1) * WINDOW)
        outs = []
        for g in range(2):
            stack = []
            sink = jnp.zeros((1, group * WINDOW), F32)
            for j in range(group):
                h = g * group + j
                q = q_ref[here, h // 2 * LANES : (h // 2 + 1) * LANES]
                if h % 2 != g:
                    q = pltpu.roll(q.astype(F32), HEAD_DIM, 1).astype(BF16)
                stack.append(q * masks[g])
                sink = sink + jnp.where(spot == j, sink_ref[h], 0.0)
            scores = lax.dot_general(
                keys, jnp.concatenate(stack, axis=0), CONTRACT_LANES, preferred_element_type=F32
            )
            scores = jnp.where(allowed, scores, -jnp.inf)
            highest = jnp.maximum(jnp.max(scores, axis=0, keepdims=True), sink)
            raised = jnp.exp(scores - highest)
            total = jnp.sum(raised, axis=0, keepdims=True) + jnp.exp(sink - highest)
            weights = (raised * (1.0 / total)).astype(BF16)
            out = lax.dot_general(values, weights, CONTRACT_ROWS, preferred_element_type=F32)
            out = out[g * HEAD_DIM : (g + 1) * HEAD_DIM]
            outs += [out[:, j * WINDOW : (j + 1) * WINDOW] for j in range(group)]
        for p in range(heads // 2):
            both = jnp.concatenate([outs[2 * p], outs[2 * p + 1]], axis=0)
            out_ref[here, p * LANES : (p + 1) * LANES] = both.T.astype(BF16)


def window(mine, side, spot, q, kv, halo, sinks):
    rows, width = q.shape
    return call(
        functools.partial(window_body, mine),
        [
            pl.BlockSpec((rows // 2, width), lambda i, t, f: (half_of(t, mine), 0)),
            whole(kv.shape),
            whole(halo.shape),
            pl.BlockSpec(memory_space=pltpu.SMEM),
        ],
        whole((rows // 2, width)),
        jax.ShapeDtypeStruct((rows // 2, width), BF16),
        [pltpu.VMEM((rows // 2 + WINDOW, kv.shape[1]), BF16)],
        2,
        2**30,
        8,
        "window",
    )(side, spot, q, kv, halo, sinks)


def first_exit_body(a, b, wa, wb, out):
    rows = jnp.concatenate([a[...], b[...]], axis=1)
    for n in range(0, out.shape[1], CHUNK):
        here = slice(n, n + CHUNK)
        out[:, here] = dot(rows, jnp.concatenate([wa[:, here], wb[:, here]], axis=0))


def last_exit_body(a, b, wa, wb, more, out, buffer, sems):
    rows = jnp.concatenate([a[...], b[...]], axis=1)
    copies = []
    for i, n in enumerate(range(0, out.shape[1], 2 * CHUNK)):
        for m in (n, n + CHUNK):
            here = slice(m, m + CHUNK)
            part = dot(rows, jnp.concatenate([wa[:, here], wb[:, here]], axis=0))
            buffer[:, here] = (more[:, here] + part).astype(BF16)
        copy = pltpu.make_async_copy(
            buffer.at[:, n : n + 2 * CHUNK], out.at[:, n : n + 2 * CHUNK], sems.at[i]
        )
        copy.start()
        copies.append(copy)
    for copy in copies:
        copy.wait()


def first_exit(a, b, wa, wb):
    args = (a, b, wa, wb)
    shape = (a.shape[0], wa.shape[1])
    return call(
        first_exit_body,
        [whole(x.shape) for x in args],
        whole(shape),
        jax.ShapeDtypeStruct(shape, F32),
        [],
        0,
        4 * a.shape[0] * a.shape[1] * wa.shape[1],
        12,
        "first_exit",
    )(*args)


def last_exit(a, b, wa, wb, more):
    args = (a, b, wa, wb, more)
    shape = (a.shape[0], wa.shape[1])
    return call(
        last_exit_body,
        [whole(x.shape) for x in args],
        IN_HBM,
        jax.ShapeDtypeStruct(shape, BF16),
        [pltpu.VMEM(shape, BF16), pltpu.SemaphoreType.DMA((shape[1] // (2 * CHUNK),))],
        0,
        4 * a.shape[0] * a.shape[1] * wa.shape[1],
        16,
        "last_exit",
    )(*args)


def turned(value, axis, by):
    peers = lax.axis_size(axis)
    return lax.ppermute(value, axis, [(i, (i + by) % peers) for i in range(peers)])


def shards(
    tokens,
    in_gain,
    ret_query,
    ret_key,
    ret_value,
    att_query,
    att_key,
    att_value,
    log_decay,
    ret_gain,
    sink_logit,
    retentive_exit_matrix,
    out_att,
):
    tp = lax.axis_index("tp").astype(jnp.int32)
    place = lax.axis_index(SP).astype(jnp.int32)
    own = tokens[0]
    gain = in_gain[None]
    side, spot = tp.reshape(1), place.reshape(1)
    peer = turned(own, "tp", 1)
    early = (ret_key, ret_value, att_key, att_value)
    rates = log_decay.reshape(log_decay.shape[1], 1, log_decay.shape[2])
    first, second, squares, row, col = own_half(
        side, own, gain, rates, early + (ret_query, att_query)
    )
    ret_k, ret_v, att_kv, inv, scaled, payload, more = keys_half(
        side, peer, gain, first, squares, col, early
    )
    sources = [turned(more, SP, 1), turned(payload, SP, 2), turned(payload, SP, 3)]
    ret_q, att_q = queries_half(side, scaled, second, inv, ret_query, att_query)
    inside = inner(ret_q, ret_k, ret_v, row, col)
    sources, inside = lax.optimization_barrier((sources, inside))
    halo = sources[0]
    near, near_log, span = scan_step((1, 2, 3), spot, payload, [], sources, "scan_one")
    sources = [turned(span, "sp_0", 1), turned(span, "sp_0", 2)]
    theirs = window(False, side, spot, att_q, att_kv, halo, sink_logit)
    att_got = turned(theirs, "tp", 1)
    sources, theirs = lax.optimization_barrier((sources, theirs))
    att_mine = window(True, side, spot, att_q, att_kv, halo, sink_logit)
    near, near_log, span = scan_step(
        (4, 8), spot, payload, [near, near_log], sources, "scan_two"
    )
    sources = [turned(span, "sp_0", 3), turned(span, "sp_0", 6)]
    out_att_peer = turned(out_att, "tp", 1)
    exit_peer = turned(retentive_exit_matrix, "tp", 1)
    partial = first_exit(att_mine, att_got, out_att, out_att_peer)
    sources, partial = lax.optimization_barrier((sources, partial))
    args = (ret_q, inside, col, ret_gain[None], near, near_log, sources)
    ret_got = turned(finish((12, 24), False, side, spot, *args), "tp", 1)
    ret_mine = finish((12, 24), True, side, spot, *args)
    mixed = last_exit(ret_mine, ret_got, retentive_exit_matrix, exit_peer, partial)
    return mixed[None]


def solution(mesh):
    finer = Mesh(
        mesh.devices.reshape(8, 4, mesh.shape["fs"], mesh.shape["tp"]), ("sp_0", "sp_1", "fs", "tp")
    )
    placed = (
        P("fs", SP, "tp"),
        P(),
        P(None, "tp"),
        P(None, "tp"),
        P(None, "tp"),
        P(None, "tp"),
        P(None, "tp"),
        P(None, "tp"),
        P("fs", "tp", SP),
        P("tp"),
        P("tp"),
        P("tp", None),
        P("tp", None),
    )
    return jax.shard_map(
        shards, mesh=finer, in_specs=placed, out_specs=P("fs", SP_TP, None), check_vma=False
    )
```

time: 156 us -> 50 us (0.32)
  blocking collectives: 74.6 us -> 0 us
  matrix products: 34.4 us -> 0 us
  Pallas kernels: 0 us -> 24.5 us
  between operations: 14.2 us -> 0.4 us
  starting transfers between devices: 9.45 us -> 19.9 us
  other arithmetic: 9.42 us -> 0 us
  local copies, waits for them, and re-layouts: 9.37 us -> 0.06 us
  waiting for transfers between devices: 3.52 us -> 5.08 us
    all_gather x3 -> x0, blocking collectives: 44.9 us -> none  [entering(): lax.all_gather(part.astype(kind), axis)]
    dot_general x13 -> x0, matrix products: 34.4 us -> none  [the longest x6 9.35 us: shards(): jnp.dot(scaled, weight, preferred_element_type=jnp.float32)]
    pallas_call x0 -> x12, Pallas kernels: none -> 24.5 us  [the longest x2 5.87 us: window(): call(functools.partial(window_body, mine), [pl.BlockSpec((rows // 2, widt...]
    all_to_all x1 -> x0, blocking collectives: 20.2 us -> none  [shards(): lax.all_to_all(ret_out, 'tp', split_axis=0, concat_axis=1, tiled=True)]
    ppermute x2 -> x12, starting transfers between devices: 4.72 us -> 19.9 us  [turned(): lax.ppermute(value, axis, [(i, (i + by) % peers) for i in range(peers)])]
    unnamed x1 -> x0, blocking collectives: 9.52 us -> none
    ppermute x2 -> x12, waiting for transfers between devices: 0.04 us -> 5.08 us  [turned(): lax.ppermute(value, axis, [(i, (i + by) % peers) for i in range(peers)])]
    all_to_all x1 -> x0, starting transfers between devices: 4.62 us -> none  [shards(): lax.all_to_all(att_out, 'tp', split_axis=0, concat_axis=1, tiled=True)]
  transfers between devices with their start and end apart: 6 -> 12, of which waited for: 1 -> 5; matrix products, arithmetic and copies ran while one was open for 31% -> 0% of each run, Pallas kernels for 0% -> 45%
where the time goes in v2:
time: 50 us; the launch traced here: 49.9 us
  Pallas kernels  24.5 us (49%)
  starting transfers between devices  19.9 us (40%)
  waiting for transfers between devices  5.08 us (10%)
    ppermute x12, starting transfers between devices, turned(): lax.ppermute(value, axis, [(i, (i + by) % peers) for i in range(peers)])  19.9 us
    pallas_call x2, Pallas kernels, window(): call(functools.partial(window_body, mine), [pl.BlockSpec((rows // 2, widt...  5.87 us
    pallas_call x1, Pallas kernels, own_half(): call(own_body, [IN_HBM] * 9, [whole(s) for s, _ in shapes], [jax.ShapeDty...  5.68 us
    ppermute x12, waiting for transfers between devices, turned(): lax.ppermute(value, axis, [(i, (i + by) % peers) for i in range(peers)])  5.08 us
    pallas_call x1, Pallas kernels, first_exit(): call(first_exit_body, [whole(x.shape) for x in args], whole(shape), jax.S...  2.79 us
    pallas_call x1, Pallas kernels, keys_half(): call(keys_body, [whole(a.shape) for a in (peer, gain, part, sq, col) + we...  2.58 us
    pallas_call x1, Pallas kernels, inner(): call(inner_body, [whole(a.shape) for a in args], whole(q.shape), jax.Shap...  2.43 us
    pallas_call x1, Pallas kernels, last_exit(): call(last_exit_body, [whole(x.shape) for x in args], IN_HBM, jax.ShapeDty...  2.19 us
  transfers between devices with their start and end apart: 12, of which 5 were waited for; matrix products, arithmetic and copies ran while one was open for 0% of the time, Pallas kernels for 45%

profile of v2, /device:TPU:1, one launch (start us, length us, event | category | flops | bytes accessed | tf_op | source)
XLA Modules:
  0.0 49.9 jit_solution(9052208758395970893)
XLA Ops:
  0.0 3.2 %collective-permute-start = (bf16[768,1024]{1,0:T(8,128)(2,1)}, bf16[768,1024]{1,0:T(8,128)(2,1)S(1)}, u32[]{:S(2)}, u32[]{:S(2)}) collective-permute-start(bf16[768,1024]{1,0:T(8,128)(2,1)} %bitcast.8), channel_id=1, source_target_pairs={{0,1},{1,0},{2,3},{3,2},{4,5},{5,4},{6,7},{7,6},{8,9},{9,8},{10,11... | collective-permute-start | bytes 4718600 | tf_op jit(solution)/shard_map/ppermute | solution.py:606
  3.2 0.5 %collective-permute-start.11 = (bf16[384,2048]{1,0:T(8,128)(2,1)}, bf16[384,2048]{1,0:T(8,128)(2,1)S(1)}, u32[]{:S(2)}, u32[]{:S(2)}) collective-permute-start(bf16[384,2048]{1,0:T(8,128)(2,1)} %wa.3), channel_id=1, source_target_pairs={{0,1},{1,0},{2,3},{3,2},{4,5},{5,4},{6,7},{7,6},{8,9},{9,8},{10,11... | collective-permute-start | bytes 4718600 | tf_op jit(solution)/shard_map/ppermute | solution.py:606
  3.7 5.7 %own_half.1 = (f32[768,1024]{1,0:T(8,128)S(1)}, f32[768,768]{1,0:T(8,128)S(1)}, f32[768,128]{1,0:T(8,128)S(1)}, f32[8,768]{1,0:T(8,128)S(1)}, f32[768,384]{1,0:T(8,128)S(1)}) custom-call(s32[1]{0:T(128)} %bitcast.tp.side, bf16[768,1024]{1,0:T(8,128)(2,1)} %bitcast.9, f32[1,2048]{1,0:T(1,128)} %bitcast.6, f32[6,1,768]{2,1,0:T(1,128)} %bitcast.10, ...), custom_call_target="tpu_custom_call" | custom-call | flops 2818572288 | bytes 1048576 | tf_op jit(solution)/shard_map/own_half/pallas_call | solution.py:181
  9.5 2.6 %keys_half.1 = (bf16[768,384]{1,0:T(8,128)(2,1)S(1)}, bf16[768,384]{1,0:T(8,128)(2,1)S(1)}, bf16[768,256]{1,0:T(8,128)(2,1)S(1)}, f32[768,128]{1,0:T(8,128)S(1)}...) custom-call(s32[1]{0:T(128)} %bitcast.tp.side, ...), custom_call_target="tpu_custom_call" | custom-call | flops 1610612736 | bytes 1048576 | tf_op jit(solution)/shard_map/keys_half/pallas_call | solution.py:262
  12.1 1.3 %collective-permute-start.2 = (bf16[208,128]{1,0:T(8,128)(2,1)S(1)}, bf16[208,128]{1,0:T(8,128)(2,1)S(1)}, u32[]{:S(2)}, u32[]{:S(2)}) collective-permute-start(bf16[208,128]{1,0:T(8,128)(2,1)S(1)} %get-tuple-element.42.own), channel_id=1, source_target_pairs={{0,16},{8,24},{16,32},{24,40},{32,48},{40,56},{48,64},{56,72},{64,... | collective-permute-start | bytes 159752 | tf_op jit(solution)/shard_map/ppermute | solution.py:606
  13.4 2.1 %collective-permute-start.3 = (bf16[208,128]{1,0:T(8,128)(2,1)S(1)}, bf16[208,128]{1,0:T(8,128)(2,1)S(1)}, u32[]{:S(2)}, u32[]{:S(2)}) collective-permute-start(bf16[208,128]{1,0:T(8,128)(2,1)S(1)} %get-tuple-element.42.own), channel_id=1, source_target_pairs={{0,24},{8,32},{16,40},{24,48},{32,56},{40,64},{48,72},{56,80},{64,... | collective-permute-start | bytes 159752 | tf_op jit(solution)/shard_map/ppermute | solution.py:606
  15.5 0.7 %collective-permute-start.1 = (bf16[464,128]{1,0:T(8,128)(2,1)S(1)}, bf16[464,128]{1,0:T(8,128)(2,1)S(1)}, u32[]{:S(2)}, u32[]{:S(2)}) collective-permute-start(bf16[464,128]{1,0:T(8,128)(2,1)S(1)} %get-tuple-element.41), channel_id=1, source_target_pairs={{0,8},{8,16},{16,24},{24,32},{32,40},{40,48},{48,56},{56,64},{64,7... | collective-permute-start | bytes 356360 | tf_op jit(solution)/shard_map/ppermute | solution.py:606
  16.2 1.5 %queries_half.1 = (bf16[768,384]{1,0:T(8,128)(2,1)S(1)}, bf16[768,384]{1,0:T(8,128)(2,1)S(1)}) custom-call(s32[1]{0:T(128)} %bitcast.tp.side, bf16[768,1024]{1,0:T(8,128)(2,1)S(1)} %get-tuple-element.37.scaled, f32[768,768]{1,0:T(8,128)S(1)} %get-tuple-element.38.part, f32[768,128]{1,0:T(8,128)S(1)} %get-tuple-element.39.inv, ...), custom_call_target="tpu_custom_call" | custom-call | flops 1207959552 | bytes 1048576 | tf_op jit(solution)/shard_map/queries_half/pallas_call | solution.py:297
  17.7 2.4 %inner.1.in_ref = f32[768,384]{1,0:T(8,128)S(1)} custom-call(bf16[768,384]{1,0:T(8,128)(2,1)S(1)} %get-tuple-element.40.q_ref, bf16[768,384]{1,0:T(8,128)(2,1)S(1)} %get-tuple-element.43.k_ref, bf16[768,384]{1,0:T(8,128)(2,1)S(1)} %get-tuple-element.44.v_ref, f32[8,768]{1,0:T(8,128)S(1)} %get-tuple-element.45.row_ref, ...), custom_call_target="tpu_custom_call" | custom-call | flops 3221225472 | bytes 1048576 | tf_op jit(solution)/shard_map/inner/pallas_call | solution.py:348
  20.2 0.7 %collective-permute-done.2.refs_1_ = bf16[208,128]{1,0:T(8,128)(2,1)S(1)} collective-permute-done((bf16[208,128]{1,0:T(8,128)(2,1)S(1)}, bf16[208,128]{1,0:T(8,128)(2,1)S(1)}, u32[]{:S(2)}, u32[]{:S(2)}) %collective-permute-start.2) | collective-permute-done | bytes 53280 | tf_op jit(solution)/shard_map/ppermute | solution.py:606
  21.0 3.0 %collective-permute-done.1.refs_0_.halo_ref = bf16[464,128]{1,0:T(8,128)(2,1)S(1)} collective-permute-done((bf16[464,128]{1,0:T(8,128)(2,1)S(1)}, bf16[464,128]{1,0:T(8,128)(2,1)S(1)}, u32[]{:S(2)}, u32[]{:S(2)}) %collective-permute-start.1) | collective-permute-done | bytes 118816 | tf_op jit(solution)/shard_map/ppermute | solution.py:606
  24.0 2.9 %window.2 = bf16[384,384]{1,0:T(8,128)(2,1)S(1)} custom-call(s32[1]{0:T(128)} %bitcast.tp.side, s32[1]{0:T(128)} %bitcast.1.where.spot, bf16[768,384]{1,0:T(8,128)(2,1)S(1)} %get-tuple-element.53.q_ref, bf16[768,256]{1,0:T(8,128)(2,1)S(1)} %get-tuple-element.54.kv_ref, bf16[464,128]{1,0:T(8,128)(2,1)S(1)} %collective-permute-done.1.refs_0_.halo_ref, ...), custom_call_target="tpu_custom_call" | custom-call | flops 1073741824 | bytes 1048576 | tf_op jit(solution)/shard_map/window/pallas_call | solution.py:530
  27.0 1.0 %collective-permute-start.8 = (bf16[384,384]{1,0:T(8,128)(2,1)S(1)}, bf16[384,384]{1,0:T(8,128)(2,1)S(1)}, u32[]{:S(2)}, u32[]{:S(2)}) collective-permute-start(bf16[384,384]{1,0:T(8,128)(2,1)S(1)} %window.2), channel_id=1, source_target_pairs={{0,1},{1,0},{2,3},{3,2},{4,5},{5,4},{6,7},{7,6},{8,9},{9,8},{10,11... | collective-permute-start | bytes 884744 | tf_op jit(solution)/shard_map/ppermute | solution.py:606
  28.2 4.1 %collective-permute-start.5 = (bf16[208,128]{1,0:T(8,128)(2,1)S(1)}, bf16[208,128]{1,0:T(8,128)(2,1)S(1)}, u32[]{:S(2)}, u32[]{:S(2)}) collective-permute-start(bf16[208,128]{1,0:T(8,128)(2,1)S(1)} %get-tuple-element.52), channel_id=1, source_target_pairs={{0,64},{32,96},{64,128},{96,160},{128,192},{160,224},{192,0},{224,... | collective-permute-start | bytes 159752 | tf_op jit(solution)/shard_map/ppermute | solution.py:606
  32.3 2.9 %window.3.a = bf16[384,384]{1,0:T(8,128)(2,1)S(1)} custom-call(s32[1]{0:T(128)} %bitcast.tp.side, s32[1]{0:T(128)} %bitcast.1.where.spot, bf16[768,384]{1,0:T(8,128)(2,1)S(1)} %get-tuple-element.53.q_ref, bf16[768,256]{1,0:T(8,128)(2,1)S(1)} %get-tuple-element.54.kv_ref, bf16[464,128]{1,0:T(8,128)(2,1)S(1)} %collective-permute-done.1.refs_0_.halo_ref, ...), custom_call_target="tpu_custom_call" | custom-call | flops 1073741824 | bytes 1048576 | tf_op jit(solution)/shard_map/window/pallas_call | solution.py:530
  35.3 4.0 %collective-permute-start.6 = (bf16[208,128]{1,0:T(8,128)(2,1)S(1)}, bf16[208,128]{1,0:T(8,128)(2,1)S(1)}, u32[]{:S(2)}, u32[]{:S(2)}) collective-permute-start(bf16[208,128]{1,0:T(8,128)(2,1)S(1)} %get-tuple-element.59), channel_id=1, source_target_pairs={{0,96},{32,128},{64,160},{96,192},{128,224},{160,0},{192,32},{224,... | collective-permute-start | bytes 159752 | tf_op jit(solution)/shard_map/ppermute | solution.py:606
  39.3 1.3 %collective-permute-start.7 = (bf16[208,128]{1,0:T(8,128)(2,1)S(1)}, bf16[208,128]{1,0:T(8,128)(2,1)S(1)}, u32[]{:S(2)}, u32[]{:S(2)}) collective-permute-start(bf16[208,128]{1,0:T(8,128)(2,1)S(1)} %get-tuple-element.59), channel_id=1, source_target_pairs={{0,192},{32,224},{64,0},{96,32},{128,64},{160,96},{192,128},{224,1... | collective-permute-start | bytes 159752 | tf_op jit(solution)/shard_map/ppermute | solution.py:606
  40.7 2.8 %first_exit.1.more = f32[384,2048]{1,0:T(8,128)S(1)} custom-call(bf16[384,384]{1,0:T(8,128)(2,1)S(1)} %window.3.a, bf16[384,384]{1,0:T(8,128)(2,1)S(1)} %collective-permute-done.8.b, bf16[384,2048]{1,0:T(8,128)(2,1)S(1)} %copy-done.3, bf16[384,2048]{1,0:T(8,128)(2,1)} %collective-permute-done.9.wb), custom_call_target="tpu_custom_call" | custom-call | flops 1207959552 | bytes 1048576 | tf_op jit(solution)/shard_map/first_exit/pallas_call | solution.py:575
  43.5 0.7 %collective-permute-done.7.refs_1_ = bf16[208,128]{1,0:T(8,128)(2,1)S(1)} collective-permute-done((bf16[208,128]{1,0:T(8,128)(2,1)S(1)}, bf16[208,128]{1,0:T(8,128)(2,1)S(1)}, u32[]{:S(2)}, u32[]{:S(2)}) %collective-permute-start.7) | collective-permute-done | bytes 53280 | tf_op jit(solution)/shard_map/ppermute | solution.py:606
  44.1 0.6 %finish.3 = bf16[384,384]{1,0:T(8,128)(2,1)S(1)} custom-call(s32[1]{0:T(128)} %bitcast.tp.side, s32[1]{0:T(128)} %bitcast.1.where.spot, bf16[768,384]{1,0:T(8,128)(2,1)S(1)} %get-tuple-element.40.q_ref, f32[768,384]{1,0:T(8,128)S(1)} %inner.1.in_ref, f32[768,384]{1,0:T(8,128)S(1)} %get-tuple-element.36.col.col_ref, f32[1,384]{1,0:T(1,128)S(1)} %broadcast_in_dim.10.gain, ...), custom_call_target="tpu_custom_call" | custom-call | flops 536870912 | bytes 1048576 | tf_op jit(solution)/shard_map/finish/pallas_call | solution.py:453
  44.8 1.5 %collective-permute-start.10 = (bf16[384,384]{1,0:T(8,128)(2,1)S(1)}, bf16[384,384]{1,0:T(8,128)(2,1)S(1)}, u32[]{:S(2)}, u32[]{:S(2)}) collective-permute-start(bf16[384,384]{1,0:T(8,128)(2,1)S(1)} %finish.3), channel_id=1, source_target_pairs={{0,1},{1,0},{2,3},{3,2},{4,5},{5,4},{6,7},{7,6},{8,9},{9,8},{10,11... | collective-permute-start | bytes 884744 | tf_op jit(solution)/shard_map/ppermute | solution.py:606
  46.3 0.6 %finish.2.a = bf16[384,384]{1,0:T(8,128)(2,1)S(1)} custom-call(s32[1]{0:T(128)} %bitcast.tp.side, s32[1]{0:T(128)} %bitcast.1.where.spot, bf16[768,384]{1,0:T(8,128)(2,1)S(1)} %get-tuple-element.40.q_ref, f32[768,384]{1,0:T(8,128)S(1)} %inner.1.in_ref, f32[768,384]{1,0:T(8,128)S(1)} %get-tuple-element.36.col.col_ref, f32[1,384]{1,0:T(1,128)S(1)} %broadcast_in_dim.10.gain, ...), custom_call_target="tpu_custom_call" | custom-call | flops 536870912 | bytes 1048576 | tf_op jit(solution)/shard_map/finish/pallas_call | solution.py:453
  47.0 0.5 %collective-permute-done.10.b = bf16[384,384]{1,0:T(8,128)(2,1)S(1)} collective-permute-done((bf16[384,384]{1,0:T(8,128)(2,1)S(1)}, bf16[384,384]{1,0:T(8,128)(2,1)S(1)}, u32[]{:S(2)}, u32[]{:S(2)}) %collective-permute-start.10) | collective-permute-done | bytes 294944 | tf_op jit(solution)/shard_map/ppermute | solution.py:606
  47.5 2.2 %last_exit.1 = bf16[384,2048]{1,0:T(8,128)(2,1)} custom-call(bf16[384,384]{1,0:T(8,128)(2,1)S(1)} %finish.2.a, bf16[384,384]{1,0:T(8,128)(2,1)S(1)} %collective-permute-done.10.b, bf16[384,2048]{1,0:T(8,128)(2,1)S(1)} %copy-done.2, bf16[384,2048]{1,0:T(8,128)(2,1)S(1)} %collective-permute-done.11.wb, f32[384,2048]{1,0:T(8,128)S(1)} %first_exit.1.more), custom_call_target="tpu_custom_call" | custom-call | flops 1207959552 | bytes 1048576 | tf_op jit(solution)/shard_map/last_exit/pallas_call | solution.py:591
  (35 shorter events, 0.4 us)
Async XLA Ops:
  0.0 9.4 %collective-permute-start = (bf16[768,1024]{1,0:T(8,128)(2,1)}, bf16[768,1024]{1,0:T(8,128)(2,1)S(1)}, u32[]{:S(2)}, u32[]{:S(2)}) collective-permute-start(bf16[768,1024]{1,0:T(8,128)(2,1)} %bitcast.8), channel_id=1, source_target_pairs={{0,1},{1,0},{2,3},{3,2},{4,5},{5,4},{6,7},{7,6},{8,9},{9,8},{10,11... | collective-permute-start | bytes 4718600 | tf_op jit(solution)/shard_map/ppermute | solution.py:606
  3.2 37.5 %collective-permute-start.9 = (bf16[384,2048]{1,0:T(8,128)(2,1)}, bf16[384,2048]{1,0:T(8,128)(2,1)}, u32[]{:S(2)}, u32[]{:S(2)}) collective-permute-start(bf16[384,2048]{1,0:T(8,128)(2,1)} %wa.2), channel_id=1, source_target_pairs={{0,1},{1,0},{2,3},{3,2},{4,5},{5,4},{6,7},{7,6},{8,9},{9,8},{10,11... | collective-permute-start | bytes 4718600 | tf_op jit(solution)/shard_map/ppermute | solution.py:606
  3.2 43.7 %collective-permute-start.11 = (bf16[384,2048]{1,0:T(8,128)(2,1)}, bf16[384,2048]{1,0:T(8,128)(2,1)S(1)}, u32[]{:S(2)}, u32[]{:S(2)}) collective-permute-start(bf16[384,2048]{1,0:T(8,128)(2,1)} %wa.3), channel_id=1, source_target_pairs={{0,1},{1,0},{2,3},{3,2},{4,5},{5,4},{6,7},{7,6},{8,9},{9,8},{10,11... | collective-permute-start | bytes 4718600 | tf_op jit(solution)/shard_map/ppermute | solution.py:606
  3.7 5.7 %copy-start = (bf16[2048,384]{1,0:T(8,128)(2,1)S(1)}, bf16[2048,384]{1,0:T(8,128)(2,1)}, u32[]{:S(2)}) copy-start(bf16[2048,384]{1,0:T(8,128)(2,1)} %refs_0_.3) | copy-start | bytes 4718596
  3.7 5.7 %copy-start.1 = (bf16[2048,384]{1,0:T(8,128)(2,1)S(1)}, bf16[2048,384]{1,0:T(8,128)(2,1)}, u32[]{:S(2)}) copy-start(bf16[2048,384]{1,0:T(8,128)(2,1)} %refs_1_.3) | copy-start | bytes 4718596
  3.7 5.7 %copy-start.6 = (bf16[2048,128]{1,0:T(8,128)(2,1)S(1)}, bf16[2048,128]{1,0:T(8,128)(2,1)}, u32[]{:S(2)}) copy-start(bf16[2048,128]{1,0:T(8,128)(2,1)} %refs_2_.3) | copy-start | bytes 1572868
  3.7 5.7 %copy-start.7 = (bf16[2048,128]{1,0:T(8,128)(2,1)S(1)}, bf16[2048,128]{1,0:T(8,128)(2,1)}, u32[]{:S(2)}) copy-start(bf16[2048,128]{1,0:T(8,128)(2,1)} %refs_3_.3) | copy-start | bytes 1572868
  3.7 5.7 %copy-start.8 = (f32[2048]{0:T(1024)S(1)}, f32[2048]{0:T(1024)}, u32[]{:S(2)}) copy-start(f32[2048]{0:T(1024)} %param.14) | copy-start | bytes 24580
  9.5 6.7 %copy-start.4 = (bf16[2048,384]{1,0:T(8,128)(2,1)S(1)}, bf16[2048,384]{1,0:T(8,128)(2,1)}, u32[]{:S(2)}) copy-start(bf16[2048,384]{1,0:T(8,128)(2,1)} %w0.1) | copy-start | bytes 4718596
  9.5 6.7 %copy-start.5 = (bf16[2048,384]{1,0:T(8,128)(2,1)S(1)}, bf16[2048,384]{1,0:T(8,128)(2,1)}, u32[]{:S(2)}) copy-start(bf16[2048,384]{1,0:T(8,128)(2,1)} %w1.1) | copy-start | bytes 4718596
  12.1 8.8 %collective-permute-start.2 = (bf16[208,128]{1,0:T(8,128)(2,1)S(1)}, bf16[208,128]{1,0:T(8,128)(2,1)S(1)}, u32[]{:S(2)}, u32[]{:S(2)}) collective-permute-start(bf16[208,128]{1,0:T(8,128)(2,1)S(1)} %get-tuple-element.42.own), channel_id=1, source_target_pairs={{0,16},{8,24},{16,32},{24,40},{32,48},{40,56},{48,64},{56,72},{64,... | collective-permute-start | bytes 159752 | tf_op jit(solution)/shard_map/ppermute | solution.py:606
  13.4 7.6 %collective-permute-start.3 = (bf16[208,128]{1,0:T(8,128)(2,1)S(1)}, bf16[208,128]{1,0:T(8,128)(2,1)S(1)}, u32[]{:S(2)}, u32[]{:S(2)}) collective-permute-start(bf16[208,128]{1,0:T(8,128)(2,1)S(1)} %get-tuple-element.42.own), channel_id=1, source_target_pairs={{0,24},{8,32},{16,40},{24,48},{32,56},{40,64},{48,72},{56,80},{64,... | collective-permute-start | bytes 159752 | tf_op jit(solution)/shard_map/ppermute | solution.py:606
  15.5 8.5 %collective-permute-start.1 = (bf16[464,128]{1,0:T(8,128)(2,1)S(1)}, bf16[464,128]{1,0:T(8,128)(2,1)S(1)}, u32[]{:S(2)}, u32[]{:S(2)}) collective-permute-start(bf16[464,128]{1,0:T(8,128)(2,1)S(1)} %get-tuple-element.41), channel_id=1, source_target_pairs={{0,8},{8,16},{16,24},{24,32},{32,40},{40,48},{48,56},{56,64},{64,7... | collective-permute-start | bytes 356360 | tf_op jit(solution)/shard_map/ppermute | solution.py:606
  17.7 6.3 %copy-start.9 = (f32[6]{0:T(128)S(1)}, f32[6]{0:T(128)}, u32[]{:S(2)}) copy-start(f32[6]{0:T(128)} %sink_ref.3) | copy-start | bytes 76
  24.0 4.0 %copy-start.10 = (f32[384]{0:T(512)S(1)}, f32[384]{0:T(512)}, u32[]{:S(2)}) copy-start(f32[384]{0:T(512)} %param.22) | copy-start | bytes 4612
  27.0 13.7 %collective-permute-start.8 = (bf16[384,384]{1,0:T(8,128)(2,1)S(1)}, bf16[384,384]{1,0:T(8,128)(2,1)S(1)}, u32[]{:S(2)}, u32[]{:S(2)}) collective-permute-start(bf16[384,384]{1,0:T(8,128)(2,1)S(1)} %window.2), channel_id=1, source_target_pairs={{0,1},{1,0},{2,3},{3,2},{4,5},{5,4},{6,7},{7,6},{8,9},{9,8},{10,11... | collective-permute-start | bytes 884744 | tf_op jit(solution)/shard_map/ppermute | solution.py:606
  28.1 12.6 %copy-start.3 = (bf16[384,2048]{1,0:T(8,128)(2,1)S(1)}, bf16[384,2048]{1,0:T(8,128)(2,1)}, u32[]{:S(2)}) copy-start(bf16[384,2048]{1,0:T(8,128)(2,1)} %wa.2) | copy-start | bytes 4718596
  28.1 7.2 %collective-permute-start.4 = (bf16[208,128]{1,0:T(8,128)(2,1)S(1)}, bf16[208,128]{1,0:T(8,128)(2,1)S(1)}, u32[]{:S(2)}, u32[]{:S(2)}) collective-permute-start(bf16[208,128]{1,0:T(8,128)(2,1)S(1)} %get-tuple-element.52), channel_id=1, source_target_pairs={{0,32},{32,64},{64,96},{96,128},{128,160},{160,192},{192,224},{224... | collective-permute-start | bytes 159752 | tf_op jit(solution)/shard_map/ppermute | solution.py:606
  28.2 7.1 %collective-permute-start.5 = (bf16[208,128]{1,0:T(8,128)(2,1)S(1)}, bf16[208,128]{1,0:T(8,128)(2,1)S(1)}, u32[]{:S(2)}, u32[]{:S(2)}) collective-permute-start(bf16[208,128]{1,0:T(8,128)(2,1)S(1)} %get-tuple-element.52), channel_id=1, source_target_pairs={{0,64},{32,96},{64,128},{96,160},{128,192},{160,224},{192,0},{224,... | collective-permute-start | bytes 159752 | tf_op jit(solution)/shard_map/ppermute | solution.py:606
  35.3 8.1 %collective-permute-start.6 = (bf16[208,128]{1,0:T(8,128)(2,1)S(1)}, bf16[208,128]{1,0:T(8,128)(2,1)S(1)}, u32[]{:S(2)}, u32[]{:S(2)}) collective-permute-start(bf16[208,128]{1,0:T(8,128)(2,1)S(1)} %get-tuple-element.59), channel_id=1, source_target_pairs={{0,96},{32,128},{64,160},{96,192},{128,224},{160,0},{192,32},{224,... | collective-permute-start | bytes 159752 | tf_op jit(solution)/shard_map/ppermute | solution.py:606
  39.3 4.8 %collective-permute-start.7 = (bf16[208,128]{1,0:T(8,128)(2,1)S(1)}, bf16[208,128]{1,0:T(8,128)(2,1)S(1)}, u32[]{:S(2)}, u32[]{:S(2)}) collective-permute-start(bf16[208,128]{1,0:T(8,128)(2,1)S(1)} %get-tuple-element.59), channel_id=1, source_target_pairs={{0,192},{32,224},{64,0},{96,32},{128,64},{160,96},{192,128},{224,1... | collective-permute-start | bytes 159752 | tf_op jit(solution)/shard_map/ppermute | solution.py:606
  44.8 2.7 %copy-start.2 = (bf16[384,2048]{1,0:T(8,128)(2,1)S(1)}, bf16[384,2048]{1,0:T(8,128)(2,1)}, u32[]{:S(2)}) copy-start(bf16[384,2048]{1,0:T(8,128)(2,1)} %wa.3) | copy-start | bytes 4718596
  44.8 2.7 %collective-permute-start.10 = (bf16[384,384]{1,0:T(8,128)(2,1)S(1)}, bf16[384,384]{1,0:T(8,128)(2,1)S(1)}, u32[]{:S(2)}, u32[]{:S(2)}) collective-permute-start(bf16[384,384]{1,0:T(8,128)(2,1)S(1)} %finish.3), channel_id=1, source_target_pairs={{0,1},{1,0},{2,3},{3,2},{4,5},{5,4},{6,7},{7,6},{8,9},{9,8},{10,11... | collective-permute-start | bytes 884744 | tf_op jit(solution)/shard_map/ppermute | solution.py:606
